TPU v7x, 256 devices: a whole 4x4x8 slice. The times are simulated.
256 devices in a mesh: sp: 16 (over y, x), tp: 16 (over z, core).
Axes of the slice: x: 4, y: 4, z: 8, core: 2. Of those that a mesh axis runs over, the one named last changes fastest.
Arguments:
- queries: bfloat16 [6144, 2048], P('sp', 'tp'), may hold values from -6 to 6
- cell_key_rows: bfloat16 [6144, 2048], P('sp', 'tp'), may hold values from -6 to 6
- cell_value_rows: bfloat16 [6144, 2048], P('sp', 'tp'), may hold values from -6 to 6
- output_gate_logits: bfloat16 [6144, 2048], P('sp', 'tp'), may hold values from -6 to 6
- input_gate_logs: float32 [16, 6144], P('tp', 'sp'), may hold values from -5 to 250
- forget_gate_logits: float32 [16, 6144], P('tp', 'sp'), may hold values from 1 to 13
- extra_log_forget: float32 [16, 6144], P('tp', 'sp'), may hold values from -0.7 to 0
- head_norm_gain: float32 [2048], P('tp'), may hold values from 0.1 to 1.9
- cell_output_matrix: bfloat16 [2048, 4096], P('tp'), may hold values from -0.125 to 0.125
- residual: bfloat16 [6144, 4096], P('sp'), may hold values from -6 to 6
- expert_norm_gain: float32 [4096], replicated, may hold values from 0.1 to 1.9
- routes: int32 [6144, 2], P('sp'), may hold values from 0 to 15, all different within a row; in each aligned block of 24 rows (0 to 23, 24 to 47, ...) at most 6 rows name the same one
- token_expert_weights: float32 [6144, 2], P('sp'), may hold values from 0.2 to 1
- expert_gate_matrix: bfloat16 [16, 4096, 2048], P('sp', None, 'tp'), may hold values from -0.09375 to 0.09375
- expert_up_matrix: bfloat16 [16, 4096, 2048], P('sp', None, 'tp'), may hold values from -0.09375 to 0.09375
- expert_down_matrix: bfloat16 [16, 2048, 4096], P('sp', 'tp'), may hold values from -0.125 to 0.125
Outputs:
- layer_out: bfloat16 [6144, 4096], P(('sp', 'tp'))
Inputs may be any that keep to these rules, and one draw needn't show every extreme that they name: `routes`: each row names 2 different experts. In the rows of one device (aligned blocks of 24 rows) no expert is named more than 6 times, and in some blocks one expert is named exactly 6 times.
All inputs are finite; a program needn't handle non-finite values.
Results may differ from a plain program's by a relative error of at most 0.019.
Values may be sent and summed in bfloat16 or wider, within the bound.
A program may use at most 128 MiB of HBM per device.

v0:
```python
import jax
import jax.numpy as jnp
from jax import lax
from jax.sharding import Mesh
from jax.sharding import PartitionSpec as P

HEAD_DIM = 128
BLOCK = 128
TP = ("tp_0", "tp_1")
SP_TP = ("sp", "tp_0", "tp_1")


floor_neg = -1e30
norm_eps = 1e-06


def from_everyone(x, axis):
    count = lax.axis_size(axis)
    return lax.all_to_all(jnp.broadcast_to(x[None], (count, *x.shape)), axis, 0, 0, tiled=True)


def all_in_one(x, axis):
    leaves = jax.tree.leaves(x)
    order = sorted(range(len(leaves)), key=lambda k: -leaves[k].size)
    width = (1, *leaves[order[0]].shape)[-1]
    lines = [
        jnp.pad(leaves[k].reshape(-1), (0, -leaves[k].size % width)).reshape(-1, width)
        for k in order
    ]
    both, at, found = (from_everyone(jnp.concatenate(lines), axis), 0, {})
    for k, line in zip(order, lines):
        section = both[:, at : at + len(line)].reshape(len(both), -1)
        found[k] = section[:, : leaves[k].size].reshape(-1, *leaves[k].shape)
        at += len(line)
    numbers = iter(range(len(leaves)))
    return jax.tree.map(lambda _: found[next(numbers)], x)


def folded_in_pairs(pieces, combine):
    while len(jax.tree.leaves(pieces)[0]) > 1:
        pieces = jax.vmap(combine)(
            *(jax.tree.map(lambda part: part[side::2], pieces) for side in (0, 1))
        )
    return jax.tree.map(lambda part: part[0], pieces)


def prefix(x, axis, combine, identity):
    count, here = (lax.axis_size(axis), lax.axis_index(axis))
    passed = jnp.arange(count) < here

    def kept(part, zero, own):
        part = jnp.where(
            passed.reshape(-1, *(1 for _ in own.shape)), part, jnp.asarray(zero, own.dtype)
        )
        return part

    pieces = all_in_one(x, axis)
    return folded_in_pairs(jax.tree.map(kept, pieces, identity, x), combine)


def in_blocks(x, dim, count):
    before, after = (x.shape[:dim], x.shape[dim + 1 :])
    return jnp.moveaxis(x.reshape(*before, count, -1, *after), dim, 0)


def sum_by_chip(x, chips, core, dim):
    sizes = (lax.axis_size(chips), lax.axis_size(core))
    parts = in_blocks(x, dim, sizes[0] * sizes[1])
    inside = parts.shape[1:]
    parts = parts.reshape(*sizes, *inside).swapaxes(0, 1).reshape(-1, *inside)
    parts = lax.psum_scatter(parts, core, scatter_dimension=0, tiled=True)
    return lax.psum_scatter(parts, chips, scatter_dimension=0, tiled=True)[0]


def block_cells(query_f, key_f, value_f, input_f, forget_log_values, start_cell, start_stab):
    heads, length, width = query_f.shape
    count = length // BLOCK
    highest = lax.Precision.HIGHEST

    def split(array):
        return jnp.moveaxis(array.reshape((heads, count, BLOCK) + array.shape[2:]), 1, 0)

    causal = jnp.tril(jnp.ones((BLOCK, BLOCK), dtype=bool))

    def advance(carry, block):
        cell, stab = carry
        qblock, kblock, vblock, iblock, fblock = block
        cumul = jnp.cumsum(fblock, axis=-1)
        total = cumul[:, -1]
        log_inner = jnp.where(
            causal[None], cumul[:, :, None] - cumul[:, None, :] + iblock[:, None, :], floor_neg
        )
        carried = cumul + stab[:, None]
        stab_row = jnp.maximum(carried, jnp.max(log_inner, axis=-1))
        scores = jnp.einsum("hld,hsd->hls", qblock, kblock, precision=highest) * jnp.exp(
            log_inner - stab_row[..., None]
        )
        numer = jnp.einsum("hls,hsd->hld", scores, vblock, precision=highest) + jnp.exp(
            carried - stab_row
        )[..., None] * jnp.einsum("hld,hde->hle", qblock, cell, precision=highest)
        log_write = total[:, None] - cumul + iblock
        stab_next = jnp.maximum(total + stab, jnp.max(log_write, axis=-1))
        weights = jnp.exp(log_write - stab_next[:, None])
        cell_next = jnp.exp(total + stab - stab_next)[:, None, None] * cell + jnp.einsum(
            "hsd,hse->hde", kblock * weights[..., None], vblock, precision=highest
        )
        return ((cell_next, stab_next), (numer, stab_row))

    inputs = tuple(
        (split(array) for array in (query_f, key_f, value_f, input_f, forget_log_values))
    )
    unused, (numer, stab_rows) = lax.scan(advance, (start_cell, start_stab), inputs)
    numer = jnp.moveaxis(numer, 0, 1).reshape(heads, length, width)
    stab_rows = jnp.moveaxis(stab_rows, 0, 1).reshape(heads, length)
    return (numer, stab_rows)


def combine_states(earlier, later):
    cell_early, stab_early, total_early = earlier
    cell_late, stab_late, total_late = later
    stab = jnp.maximum(total_late + stab_early, stab_late)
    cell = (
        jnp.exp(total_late + stab_early - stab)[:, None, None] * cell_early
        + jnp.exp(stab_late - stab)[:, None, None] * cell_late
    )
    return (cell, stab, total_early + total_late)


def rms_scale(rows, gain):
    values = rows.astype(jnp.float32)
    return (
        values * lax.rsqrt(jnp.mean(values * values, axis=-1, keepdims=True) + norm_eps) * gain
    ).astype(jnp.bfloat16)


def slot_tables(block_routes, experts, capacity):
    flat = block_routes.reshape(-1)
    count = flat.shape[0]
    topk = block_routes.shape[1]
    onehot = (flat[:, None] == jnp.arange(experts, dtype=jnp.int32)[None, :]).astype(jnp.int32)
    before = jnp.cumsum(onehot, axis=0) - onehot
    position = jnp.sum(before * onehot, axis=1)
    slot = flat * capacity + position
    match = slot[None, :] == jnp.arange(experts * capacity, dtype=jnp.int32)[:, None]
    owner = jnp.arange(count, dtype=jnp.int32)[None, :] // topk + 1
    source = jnp.sum(jnp.where(match, owner, 0), axis=1) - 1
    return (slot, source)


def fill_slots(rows, source):
    picked = rows[jnp.maximum(source, 0)]
    return jnp.where((source >= 0)[:, None], picked, jnp.zeros_like(picked))


def local(
    queries,
    cell_key_rows,
    cell_value_rows,
    output_gate_logits,
    input_gate_logs,
    forget_gate_logits,
    extra_log_forget,
    head_norm_gain,
    cell_output_matrix,
    residual,
    expert_norm_gain,
    routes,
    token_expert_weights,
    expert_gate_matrix,
    expert_up_matrix,
    expert_down_matrix,
):
    length = queries.shape[0]
    heads = queries.shape[1] // HEAD_DIM
    tp_count = lax.axis_size(TP)
    experts = lax.axis_size("sp")
    topk = routes.shape[1]
    tokens = length // tp_count
    capacity = max(2, 2 * tokens * topk // experts)
    highest = lax.Precision.HIGHEST
    tp_index = lax.axis_index(TP)

    def heads_of(array):
        return jnp.transpose(array.astype(jnp.float32).reshape(length, heads, HEAD_DIM), (1, 0, 2))

    query_f = heads_of(queries)
    key_f = heads_of(cell_key_rows) * HEAD_DIM ** (-0.5)
    value_f = heads_of(cell_value_rows)
    forget_log_values = jax.nn.log_sigmoid(forget_gate_logits) + extra_log_forget
    running = jnp.cumsum(forget_log_values, axis=1)
    total_dev = running[:, -1]
    log_write = input_gate_logs + total_dev[:, None] - running
    stab_dev = jnp.max(log_write, axis=1)
    cell_dev = jnp.einsum(
        "hsd,hse->hde",
        key_f * jnp.exp(log_write - stab_dev[:, None])[..., None],
        value_f,
        precision=highest,
    )
    identity = (
        jnp.zeros_like(cell_dev),
        jnp.full_like(stab_dev, floor_neg),
        jnp.zeros_like(total_dev),
    )
    prefix_cell, prefix_stab, prefix_total = prefix(
        (cell_dev, stab_dev, total_dev), "sp", combine_states, identity
    )
    start_stab = jnp.maximum(prefix_stab, prefix_total)
    start_cell = jnp.exp(prefix_stab - start_stab)[:, None, None] * prefix_cell
    numer_local, stab_local = block_cells(
        query_f,
        key_f,
        value_f,
        input_gate_logs,
        forget_log_values,
        jnp.zeros_like(cell_dev),
        jnp.full_like(stab_dev, floor_neg),
    )
    carried = running + start_stab[:, None]
    stab_rows = jnp.maximum(stab_local, carried)
    numer = jnp.exp(stab_local - stab_rows)[..., None] * numer_local + jnp.exp(carried - stab_rows)[
        ..., None
    ] * jnp.einsum("hld,hde->hle", query_f, start_cell, precision=highest)
    scaled = (
        numer
        * lax.rsqrt(jnp.mean(numer * numer, axis=2, keepdims=True) + norm_eps)
        * head_norm_gain.reshape(heads, 1, HEAD_DIM)
    )
    mixed = jnp.transpose(scaled, (1, 0, 2)).reshape(length, heads * HEAD_DIM)
    cell_out = (jax.nn.sigmoid(output_gate_logits.astype(jnp.float32)) * mixed).astype(jnp.bfloat16)
    gate_local = expert_gate_matrix[0]
    up_local = expert_up_matrix[0]
    down_local = expert_down_matrix[0]
    projected = sum_by_chip(
        jnp.dot(cell_out, cell_output_matrix, preferred_element_type=jnp.float32).astype(
            jnp.bfloat16
        ),
        "tp_0",
        "tp_1",
        0,
    ).astype(jnp.float32)
    own_residual = lax.dynamic_slice_in_dim(residual, tp_index * tokens, tokens, 0)
    after_mix = (own_residual.astype(jnp.float32) + projected).astype(jnp.bfloat16)
    own_routes = lax.dynamic_slice_in_dim(routes, tp_index * tokens, tokens, 0)
    slot, source = slot_tables(own_routes, experts, capacity)
    moe_in = rms_scale(after_mix, expert_norm_gain)
    sent = fill_slots(moe_in, source).reshape(experts, capacity, moe_in.shape[1])
    arrived = lax.all_to_all(sent, "sp", split_axis=0, concat_axis=0, tiled=True)
    piece = lax.all_gather(arrived, TP, axis=0, tiled=True)
    gate = jnp.einsum("rcd,df->rcf", piece, gate_local, preferred_element_type=jnp.float32)
    upper = jnp.einsum("rcd,df->rcf", piece, up_local, preferred_element_type=jnp.float32)
    hidden = (jax.nn.silu(gate) * upper).astype(jnp.bfloat16)
    summed = lax.psum_scatter(
        jnp.einsum("rcf,fd->rcd", hidden, down_local, preferred_element_type=jnp.float32).astype(
            jnp.bfloat16
        ),
        TP,
        scatter_dimension=0,
        tiled=True,
    )
    returned = lax.all_to_all(summed, "sp", split_axis=0, concat_axis=0, tiled=True)
    width = returned.shape[2]
    chosen = returned.reshape(experts * capacity, width)[slot].reshape(tokens, topk, width)
    own_weight = lax.dynamic_slice_in_dim(token_expert_weights, tp_index * tokens, tokens, 0)
    moe = jnp.sum(own_weight[:, :, None] * chosen.astype(jnp.float32), axis=1)
    return (after_mix.astype(jnp.float32) + moe).astype(jnp.bfloat16)


def solution(mesh):
    torus = Mesh(mesh.devices.reshape(mesh.shape["sp"], 8, 2), ("sp", "tp_0", "tp_1"))
    in_specs = (
        P("sp", TP),
        P("sp", TP),
        P("sp", TP),
        P("sp", TP),
        P(TP, "sp"),
        P(TP, "sp"),
        P(TP, "sp"),
        P(TP),
        P(TP, None),
        P("sp", None),
        P(),
        P("sp", None),
        P("sp", None),
        P("sp", None, TP),
        P("sp", None, TP),
        P("sp", TP, None),
    )
    out_specs = P(SP_TP, None)
    return jax.shard_map(local, mesh=torus, in_specs=in_specs, out_specs=out_specs, check_vma=False)
```

profile of v0, /device:TPU:32, one launch (start us, length us, event | category | flops | bytes accessed | tf_op | source)
XLA Modules:
  0.0 362.0 jit_solution(14984561778351580982)
XLA Ops:
  8.7 2.0 fusion.76
  10.7 2.0 multiply_reduce_fusion.2
  12.8 1.3 pad_bitcast_fusion
  14.1 1.4 fusion.54
  15.5 1.1 broadcast_in_dim.64
  16.6 7.0 %all-to-all-start = ((f32[16,130,128]{2,1,0:T(8,128)}), f32[16,130,128]{2,1,0:T(8,128)S(1)}, u32[]{:S(2)}, u32[]{:S(2)}) async-start(f32[16,130,128]{2,1,0:T(8,128)} %broadcast_in_dim.64), calls=%async_computation | async-start | bytes 2228224 | tf_op jit(solution)/shard_map/all_to_all | solution.py:19
  23.7 0.9 convert_multiply_fusion.3
  26.4 21.0 %while.17 = (s32[]{:T(128)}, f32[1,128,128]{2,1,0:T(8,128)S(1)}, f32[1]{0:T(128)}, f32[3,1,128,128]{3,2,1,0:T(8,128)S(1)}, f32[3,1,128]{2,1,0:T(1,128)S(1)}, /*i...) while((s32[]{:T(128)}, f32[1,128,128]{2,1,0:T(8,128)S(1)}, ...), condition=%wide.region_4.5_spmd.clone, body=%wide.region_0.4_spmd.clone.sunk | while | flops 100975744 | bytes 934644 | solution.py:112
  27.4 2.0 fusion.116
  30.7 1.3 subtract_exponential_fusion.4
  34.4 2.0 fusion.116
  37.7 1.3 subtract_exponential_fusion.4
  41.4 2.0 fusion.116
  44.7 1.3 subtract_exponential_fusion.4
  47.5 1.0 copy.53
  55.3 2.3 convolution_convert_fusion.1
  57.6 2.0 copy.56
  59.7 19.5 %reduce-scatter.4.cloned.1.call-done = bf16[8,24,4096]{2,1,0:T(8,128)(2,1)} async-done(((bf16[16,24,4096]{2,1,0:T(8,128)(2,1)}), bf16[8,24,4096]{2,1,0:T(8,128)(2,1)}) %reduce-scatter.4.cloned.1.call-update) | async-done | bytes 1572880 | tf_op jit(solution)/shard_map/reduce_scatter | solution.py:71
  80.8 42.2 %reduce-scatter.6.cloned.1.call-done = bf16[1,24,4096]{2,1,0:T(8,128)(2,1)} async-done(((bf16[8,24,4096]{2,1,0:T(8,128)(2,1)}), bf16[1,24,4096]{2,1,0:T(8,128)(2,1)}) %reduce-scatter.6.cloned.1.call-update) | async-done | bytes 196624 | tf_op jit(solution)/shard_map/reduce_scatter | solution.py:72
  123.0 1.2 fusion.48
  124.3 1.9 gather_fusion
  126.3 1.5 gather.9
  127.9 19.8 %all_to_all.15 = bf16[16,6,4096]{2,1,0:T(8,128)(2,1)S(1)} all-to-all(bf16[16,6,4096]{2,1,0:T(8,128)(2,1)S(1)} %broadcast_select_fusion), channel_id=1, replica_groups=mesh['sp'=16,'tp_0'=8,'tp_1'=2] {'sp'}, dimensions={0} | all-to-all | bytes 1572864 | tf_op jit(solution)/shard_map/all_to_all | solution.py:248
  147.7 1.4 copy.59
  149.3 69.9 %all-gather.2.cloned.1.call-done = bf16[256,6,4096]{2,0,1:T(8,128)(2,1)} async-done(((bf16[16,6,4096]{2,0,1:T(8,128)(2,1)}), bf16[256,6,4096]{2,0,1:T(8,128)(2,1)}) %all-gather.2.cloned.1.call-update) | async-done | bytes 12582928 | tf_op jit(solution)/shard_map/all_gather | solution.py:249
  219.2 6.7 %fusion.41 = f32[256,6,128]{2,0,1:T(8,128)S(1)} fusion(bf16[256,6,4096]{2,0,1:T(8,128)(2,1)} %all-gather.2.cloned.1.call-done, bf16[1,4096,128]{2,1,0:T(8,128)(2,1)} %param.31), kind=kOutput, calls=%fused_computation.59 | convolution fusion | flops 1610612736 | bytes 14417920 | tf_op jit(solution)/shard_map/rcd,df->rcf/dot_general | solution.py:250
  225.9 18.6 %convolution_convert_fusion = bf16[256,6,4096]{2,0,1:T(8,128)(2,1)} fusion(bf16[256,6,4096]{2,0,1:T(8,128)(2,1)} %all-gather.2.cloned.1.call-done, bf16[1,128,4096]{2,1,0:T(8,128)(2,1)S(1)} %copy-done, bf16[1,4096,128]{2,1,0:T(8,128)(2,1)S(1)} %copy-done.1, f32[256,6,128]{2,0,1:T(8,128)S(1)} %fusion.41), kind=kOutput, calls=%fused_computation.48 | convolution fusion | flops 3228696576 | bytes 28049408 | tf_op jit(solution)/shard_map/rcf,fd->rcd/dot_general | solution.py:254
  244.5 77.4 %reduce-scatter.8.cloned.1.call-done = bf16[16,6,4096]{2,0,1:T(8,128)(2,1)} async-done(((bf16[256,6,4096]{2,0,1:T(8,128)(2,1)}), bf16[16,6,4096]{2,0,1:T(8,128)(2,1)}) %reduce-scatter.8.cloned.1.call-update) | async-done | bytes 786448 | tf_op jit(solution)/shard_map/reduce_scatter | solution.py:253
  321.9 2.6 copy.60
  324.5 6.8 %all-to-all-start.2 = ((bf16[16,6,4096]{2,1,0:T(8,128)(2,1)}), bf16[16,6,4096]{2,1,0:T(8,128)(2,1)S(1)}, u32[]{:S(2)}, u32[]{:S(2)}) async-start(bf16[16,6,4096]{2,1,0:T(8,128)(2,1)} %copy.60), calls=%async_computation.5 | async-start | bytes 2097152 | tf_op jit(solution)/shard_map/all_to_all | solution.py:261
  332.3 19.8 %all-to-all-done.2 = bf16[16,6,4096]{2,1,0:T(8,128)(2,1)S(1)} async-done(((bf16[16,6,4096]{2,1,0:T(8,128)(2,1)}), bf16[16,6,4096]{2,1,0:T(8,128)(2,1)S(1)}, u32[]{:S(2)}, u32[]{:S(2)}) %all-to-all-start.2) | async-done | bytes 786464 | tf_op jit(solution)/shard_map/all_to_all | solution.py:261
  353.6 1.1 multiply_reduce_fusion
  (121 shorter events, 19.1 us)
Async XLA Ops:
  6.5 219.4 %copy-start = (bf16[1,128,4096]{2,1,0:T(8,128)(2,1)S(1)}, bf16[1,128,4096]{2,1,0:T(8,128)(2,1)}, u32[]{:S(2)}) copy-start(bf16[1,128,4096]{2,1,0:T(8,128)(2,1)} %param.33) | copy-start | bytes 3145732
  6.5 48.4 %copy-start.2 = (bf16[384,128]{1,0:T(8,128)(2,1)S(1)}, bf16[384,128]{1,0:T(8,128)(2,1)}, u32[]{:S(2)}) copy-start(bf16[384,128]{1,0:T(8,128)(2,1)} %param.18) | copy-start | bytes 294916
  6.5 48.8 %copy-start.4 = (f32[128]{0:T(128)S(1)}, f32[128]{0:T(128)}, u32[]{:S(2)}) copy-start(f32[128]{0:T(128)} %param.25) | copy-start | bytes 1540
  16.6 32.0 %all-to-all-start = ((f32[16,130,128]{2,1,0:T(8,128)}), f32[16,130,128]{2,1,0:T(8,128)S(1)}, u32[]{:S(2)}, u32[]{:S(2)}) async-start(f32[16,130,128]{2,1,0:T(8,128)} %broadcast_in_dim.64), calls=%async_computation | async-start | bytes 2228224 | tf_op jit(solution)/shard_map/all_to_all | solution.py:19
  23.6 55.6 %reduce-scatter.4.cloned.1.call-start = ((), (), s32[]{:S(2)}) async-start(), calls=%async_computation.6 | async-start | bytes 4718592 | tf_op jit(solution)/shard_map/reduce_scatter | solution.py:71
  47.4 76.8 %copy-start.3 = (f32[4096]{0:T(1024)S(1)}, f32[4096]{0:T(1024)}, u32[]{:S(2)}) copy-start(f32[4096]{0:T(1024)} %param.28) | copy-start | bytes 49156
  59.7 63.3 %reduce-scatter.6.cloned.1.call-start = ((), (), s32[]{:S(2)}) async-start(), calls=%async_computation.7 | async-start | bytes 1769472 | tf_op jit(solution)/shard_map/reduce_scatter | solution.py:72
  79.2 140.0 %all-gather.2.cloned.1.call-start = ((), (), s32[]{:S(2)}) async-start(), calls=%async_computation.8 | async-start | bytes 13369344 | tf_op jit(solution)/shard_map/all_gather | solution.py:249
  126.2 99.7 %copy-start.1 = (bf16[1,4096,128]{2,1,0:T(8,128)(2,1)S(1)}, bf16[1,4096,128]{2,1,0:T(8,128)(2,1)}, u32[]{:S(2)}) copy-start(bf16[1,4096,128]{2,1,0:T(8,128)(2,1)} %param.32) | copy-start | bytes 3145732
  149.1 172.8 %reduce-scatter.8.cloned.1.call-start = ((), (), s32[]{:S(2)}) async-start(), calls=%async_computation.9 | async-start | bytes 13369344 | tf_op jit(solution)/shard_map/reduce_scatter | solution.py:253
  324.5 27.6 %all-to-all-start.2 = ((bf16[16,6,4096]{2,1,0:T(8,128)(2,1)}), bf16[16,6,4096]{2,1,0:T(8,128)(2,1)S(1)}, u32[]{:S(2)}, u32[]{:S(2)}) async-start(bf16[16,6,4096]{2,1,0:T(8,128)(2,1)} %copy.60), calls=%async_computation.5 | async-start | bytes 2097152 | tf_op jit(solution)/shard_map/all_to_all | solution.py:261
Sparse Core Ops, SparseCore 0:
  59.8 19.4 reduce-scatter.3
  81.8 41.1 reduce-scatter.5
  149.2 69.9 all-gather.1
  244.6 77.2 reduce-scatter.7
where the time goes:
time: 363 us; the launch traced here: 362 us
  waiting for transfers between devices  229 us (63%)
  matrix products  32.4 us (9%)
  other arithmetic  25.2 us (7%)
  local copies, waits for them, and re-layouts  20 us (6%)
  blocking collectives  19.8 us (5%)
  between operations  17.3 us (5%)
  starting transfers between devices  14.2 us (4%)
  loops' own time  4.26 us (1%)
    reduce_scatter x1, waiting for transfers between devices, local(): lax.psum_scatter(jnp.einsum('rcf,fd->rcd', hidden, down_local, preferred_...  77.4 us
    all_gather x1, waiting for transfers between devices, local(): piece = lax.all_gather(arrived, TP, axis=0, tiled=True)  69.9 us
    reduce_scatter x1, waiting for transfers between devices, sum_by_chip(): return lax.psum_scatter(parts, chips, scatter_dimension=0, tiled=True)[0]  42.2 us
    all_to_all x1, blocking collectives, local(): lax.all_to_all(sent, 'sp', split_axis=0, concat_axis=0, tiled=True)  19.8 us
    all_to_all x1, waiting for transfers between devices, local(): lax.all_to_all(summed, 'sp', split_axis=0, concat_axis=0, tiled=True)  19.8 us
    reduce_scatter x1, waiting for transfers between devices, sum_by_chip(): parts = lax.psum_scatter(parts, core, scatter_dimension=0, tiled=True)  19.5 us
    dot_general x1, matrix products, local(): jnp.einsum('rcf,fd->rcd', hidden, down_local, preferred_element_type=jnp....  18.6 us
  transfers between devices with their start and end apart: 6, of which 5 were waited for; matrix products, arithmetic and copies ran while one was open for 6% of the time, Pallas kernels for 0%

commit v1 on v0

v1 whole, which is shorter than its diff:
```python
import jax
import jax.numpy as jnp
from jax import lax
from jax.experimental import pallas as pl
from jax.experimental.pallas import tpu as pltpu
from jax.sharding import PartitionSpec as P

MESH = pl.DeviceIdType.MESH
F32 = jnp.float32
BF16 = jnp.bfloat16

HEAD_DIM = 128
NSP = 16
NZ = 8
LEN = 384
TOK = 24
CAP = 6
GROUPS = 8
WIDE = 512
SLOT = GROUPS * CAP
ROWS = NSP * SLOT
TROWS = GROUPS * TOK
PIECES = 4

floor_neg = -1e30
norm_eps = 1e-06


def dot(a, b):
    return jnp.dot(a, b, preferred_element_type=F32)


def two_parts(x):
    high = x.astype(BF16)
    return high, (x - high.astype(F32)).astype(BF16)


def iota(shape, dim):
    return lax.broadcasted_iota(jnp.int32, shape, dim)


def kernel(
    q_ref, k_ref, v_ref, og_ref, ig_ref, fg_ref, ex_ref, hg_ref,
    resid_ref, eng_ref, tab_ref, rowtab_ref, perm_ref,
    wo_hbm, gate_hbm, up_hbm, down_hbm,
    out_ref,
    wv, gw, dn,
    st_send, st_recv, gs, num_s, co_f, co_a, co_b, co_send, co_recv,
    pf, r1_send, r1_recv, am,
    moe, d_send, d_recv, pin, pout,
    xring, ybuf, t_send, t_recv, r2_send, r2_recv, own,
    load_sem, wx_send, wx_recv, st_ss, st_rs, co_sem, r1_ss, r1_rs,
    d_sem, x_ss, x_rs, t_ss, t_rs, r2_ss, r2_rs,
):
    sp = lax.axis_index("sp")
    tp = lax.axis_index("tp")
    core = lax.rem(tp, 2)
    z = tp // 2
    step = jnp.where(core == 0, 1, NZ - 1)
    after = lax.rem(z + step, NZ) * 2 + core
    before = lax.rem(z + NZ - step, NZ) * 2 + core
    mate = z * 2 + 1 - core

    barrier = pltpu.get_barrier_semaphore()

    @pl.loop(1, NSP)
    def _(i):
        pl.semaphore_signal(
            barrier, inc=1, device_id={"sp": lax.rem(sp + i, NSP), "tp": tp}, device_id_type=MESH
        )

    for other in (after, before, mate):
        pl.semaphore_signal(barrier, inc=1, device_id={"sp": sp, "tp": other}, device_id_type=MESH)

    loads = [
        pltpu.make_async_copy(wo_hbm, wv.at[0], load_sem.at[0]),
        pltpu.make_async_copy(gate_hbm, gw.at[0], load_sem.at[1]),
        pltpu.make_async_copy(up_hbm, gw.at[1], load_sem.at[2]),
        pltpu.make_async_copy(down_hbm, dn.at[0], load_sem.at[3]),
    ]
    for load in loads:
        load.start()

    tt = iota((LEN, LEN), 0)
    ss = iota((LEN, LEN), 1)
    causal = ss <= tt
    fg = fg_ref[...]
    f_row = jnp.minimum(fg, 0.0) - jnp.log1p(jnp.exp(-jnp.abs(fg))) + ex_ref[...]
    i_row = ig_ref[...]
    f_all = jnp.broadcast_to(f_row, (LEN, LEN))
    f_col = jnp.sum(jnp.where(ss == tt, f_all, 0.0), axis=1, keepdims=True)
    i_col = jnp.sum(
        jnp.where(ss == tt, jnp.broadcast_to(i_row, (LEN, LEN)), 0.0), axis=1, keepdims=True
    )
    c_col = jnp.sum(jnp.where(causal, f_all, 0.0), axis=1, keepdims=True)
    c_row = jnp.sum(
        jnp.where(tt <= ss, jnp.broadcast_to(f_col, (LEN, LEN)), 0.0), axis=0, keepdims=True
    )
    total = jnp.sum(f_row, axis=1, keepdims=True)
    scale = HEAD_DIM ** (-0.5)
    write = i_col + total - c_col
    stab_dev = jnp.max(write, axis=0, keepdims=True)
    kw = k_ref[...].astype(F32) * (jnp.exp(write - stab_dev) * scale)
    kw_h, kw_l = two_parts(kw)
    dims = (((0,), (0,)), ((), ()))
    v = v_ref[...]
    st_send[:HEAD_DIM] = lax.dot_general(
        kw_h, v, dims, preferred_element_type=F32
    ) + lax.dot_general(kw_l, v, dims, preferred_element_type=F32)
    st_send[HEAD_DIM:] = jnp.where(
        iota((8, HEAD_DIM), 0) == 0,
        jnp.broadcast_to(stab_dev, (8, HEAD_DIM)),
        jnp.broadcast_to(total, (8, HEAD_DIM)),
    )

    pl.semaphore_wait(barrier, NSP - 1 + 3)

    def state_copy(to, source):
        return pltpu.make_async_remote_copy(
            src_ref=st_send, dst_ref=st_recv.at[source],
            send_sem=st_ss.at[to], recv_sem=st_rs.at[source],
            device_id={"sp": to, "tp": tp}, device_id_type=MESH,
        )

    @pl.loop(sp + 1, NSP)
    def _(to):
        state_copy(to, sp).start()

    pairs = [(wo_hbm, wv.at[1]), (gate_hbm, gw.at[2]), (up_hbm, gw.at[3]), (down_hbm, dn.at[1])]
    shared = [
        pltpu.make_async_remote_copy(
            src_ref=source, dst_ref=target, send_sem=wx_send.at[i], recv_sem=wx_recv.at[i],
            device_id={"sp": sp, "tp": mate}, device_id_type=MESH,
        )
        for i, (source, target) in enumerate(pairs)
    ]
    for copy in shared:
        copy.start()

    q = q_ref[...]
    scores = lax.dot_general(
        q, k_ref[...], (((1,), (1,)), ((), ())), preferred_element_type=F32
    ) * scale
    inner = jnp.where(causal, c_col - c_row + i_row, floor_neg)
    top = jnp.max(inner, axis=1, keepdims=True)
    p_h, p_l = two_parts(scores * jnp.exp(inner - top))
    num_s[...] = dot(p_h, v) + dot(p_l, v)

    col = iota((ROWS, ROWS), 1)
    pin[...] = jnp.where(col == perm_ref[:, 0:1], 1.0, 0.0).astype(BF16)
    pout[...] = jnp.where(col == perm_ref[:, 1:2], 1.0, 0.0).astype(BF16)

    def gather_stab(i, carry):
        stab, tot = carry
        s = sp - 1 - i
        state_copy(s, s).wait_recv()
        here = st_recv[s, HEAD_DIM : HEAD_DIM + 1, :] + tot
        gs[s, 0:1, :] = here
        return jnp.maximum(stab, here), tot + st_recv[s, HEAD_DIM + 1 : HEAD_DIM + 2, :]

    stab0, tot0 = lax.fori_loop(
        0, sp, gather_stab,
        (jnp.full((1, HEAD_DIM), floor_neg, F32), jnp.zeros((1, HEAD_DIM), F32)),
    )
    start_stab = jnp.maximum(stab0, tot0)

    def add_state(s, cell):
        return cell + jnp.exp(gs[s, 0:1, :] - start_stab) * st_recv[s, :HEAD_DIM, :]

    cell_h, cell_l = two_parts(
        lax.fori_loop(0, sp, add_state, jnp.zeros((HEAD_DIM, HEAD_DIM), F32))
    )
    carried = c_col + start_stab[:, 0:1]
    stab = jnp.maximum(top, carried)
    numer = jnp.exp(top - stab) * num_s[...] + jnp.exp(carried - stab) * (
        dot(q, cell_h) + dot(q, cell_l)
    )
    scaled = (
        numer
        * lax.rsqrt(jnp.mean(numer * numer, axis=1, keepdims=True) + norm_eps)
        * hg_ref[...]
    )
    co_f[...] = scaled / (1.0 + jnp.exp(-og_ref[...].astype(F32)))
    for i in range(NZ):
        mine = pl.multiple_of((2 * i + core) * TOK, 8)
        theirs = pl.multiple_of((2 * i + 1 - core) * TOK, 8)
        co_a[i * TOK : (i + 1) * TOK, :] = co_f[pl.ds(mine, TOK), :]
        co_b[i * TOK : (i + 1) * TOK, :] = co_f[pl.ds(theirs, TOK), :]
    co_send[...] = co_b[...].astype(BF16)
    swap = pltpu.make_async_remote_copy(
        src_ref=co_send, dst_ref=co_recv, send_sem=co_sem.at[0], recv_sem=co_sem.at[1],
        device_id={"sp": sp, "tp": mate}, device_id_type=MESH,
    )
    swap.start()
    mine_b = co_a[...].astype(BF16)

    @pl.loop(sp + 1, NSP)
    def _(to):
        state_copy(to, sp).wait_send()

    loads[0].wait()
    shared[0].wait()
    swap.wait()
    theirs_b = co_recv[...]

    @pl.loop(0, GROUPS)
    def _(j):
        at = pl.ds(pl.multiple_of(j * WIDE, WIDE), WIDE)
        part = dot(mine_b, wv[0, :, at]) + dot(theirs_b, wv[1, :, at])
        for i in range(NZ):
            pf[i, pl.ds(pl.multiple_of(j * TOK, 8), TOK), :] = part[i * TOK : (i + 1) * TOK]

    prows = TROWS // PIECES

    def sum_copy(k, p):
        rows = pl.ds(pl.multiple_of(p * prows, prows), prows)
        return pltpu.make_async_remote_copy(
            src_ref=r1_send.at[k, rows], dst_ref=r1_recv.at[k + 1, rows],
            send_sem=r1_ss.at[k, p], recv_sem=r1_rs.at[k + 1, p],
            device_id={"sp": sp, "tp": after}, device_id_type=MESH,
        )

    def block_of(k):
        return lax.rem(z + NZ * NZ - step * k, NZ)

    @pl.loop(1, NZ)
    def _(k):
        block = block_of(k)

        @pl.loop(0, PIECES)
        def _(p):
            rows = pl.ds(pl.multiple_of(p * prows, prows), prows)

            @pl.when(k == 1)
            def _():
                r1_send[k, rows] = pf[block, rows].astype(BF16)

            @pl.when(k > 1)
            def _():
                sum_copy(k - 1, p).wait_recv()
                r1_send[k, rows] = (pf[block, rows] + r1_recv[k, rows].astype(F32)).astype(BF16)

            sum_copy(k, p).start()

    @pl.loop(0, PIECES)
    def _(p):
        sum_copy(NZ - 1, p).wait_recv()

    am[...] = (resid_ref[...].astype(F32) + (pf[z] + r1_recv[NZ].astype(F32))).astype(BF16)

    squares = jnp.zeros((TOK, 1), F32)
    for j in range(GROUPS):
        x = am[...].astype(F32)[j * TOK : (j + 1) * TOK]
        squares = squares + jnp.sum(x * x, axis=1, keepdims=True)
    factor = lax.rsqrt(squares * (1.0 / (GROUPS * WIDE)) + norm_eps)
    moe[...] = jnp.concatenate(
        [
            am[...].astype(F32)[j * TOK : (j + 1) * TOK] * factor * eng_ref[j : j + 1, :]
            for j in range(GROUPS)
        ],
        axis=0,
    ).astype(BF16)
    place = iota((ROWS, TROWS), 0).astype(F32)
    pick = jnp.where(
        (place == rowtab_ref[0:1, :]) | (place == rowtab_ref[1:2, :]), 1.0, 0.0
    ).astype(BF16)
    d_send[...] = dot(pick, moe[...]).astype(BF16)

    def slot_rows(s):
        return pl.ds(pl.multiple_of(s * SLOT, SLOT), SLOT)

    @pl.loop(1, NSP)
    def _(i):
        to = lax.rem(sp + i, NSP)
        pltpu.make_async_remote_copy(
            src_ref=d_send.at[slot_rows(to)], dst_ref=d_recv.at[slot_rows(sp)],
            send_sem=d_sem.at[0], recv_sem=d_sem.at[1],
            device_id={"sp": to, "tp": tp}, device_id_type=MESH,
        ).start()

    d_recv[slot_rows(sp)] = d_send[slot_rows(sp)]

    for load in loads[1:]:
        load.wait()
    for copy in shared[1:]:
        copy.wait()

    others = pl.ds(0, ROWS - SLOT)
    for i in range(2):
        pltpu.make_async_copy(d_recv.at[others], d_recv.at[others], d_sem.at[i]).wait()
    xring[0] = dot(pin[...], d_recv[...]).astype(BF16)

    xrows = ROWS // PIECES
    per = ROWS // GROUPS

    def row_copy(k, p):
        rows = pl.ds(pl.multiple_of(p * xrows, xrows), xrows)
        return pltpu.make_async_remote_copy(
            src_ref=xring.at[k, rows], dst_ref=xring.at[k + 1, rows],
            send_sem=x_ss.at[k, p], recv_sem=x_rs.at[k, p],
            device_id={"sp": sp, "tp": after}, device_id_type=MESH,
        )

    def total_copy(k):
        return pltpu.make_async_remote_copy(
            src_ref=r2_send.at[k], dst_ref=r2_recv.at[k + 1],
            send_sem=r2_ss.at[k], recv_sem=r2_rs.at[k + 1],
            device_id={"sp": sp, "tp": after}, device_id_type=MESH,
        )

    def experts(k):
        acc = jnp.zeros((per, 4 * HEAD_DIM), F32)
        for j in range(GROUPS):
            x = xring[k, j * per : (j + 1) * per, :]
            w = jnp.concatenate([gw[i, j * WIDE : (j + 1) * WIDE, :] for i in range(4)], axis=1)
            acc = acc + dot(x, w)
        acts = []
        for i in range(2):
            gate = acc[:, 2 * i * HEAD_DIM : (2 * i + 1) * HEAD_DIM]
            upper = acc[:, (2 * i + 1) * HEAD_DIM : (2 * i + 2) * HEAD_DIM]
            acts.append((gate / (1.0 + jnp.exp(-gate)) * upper).astype(BF16))
        for j in range(GROUPS):
            at = slice(j * WIDE, (j + 1) * WIDE)
            ybuf[j * per : (j + 1) * per, :] = (
                dot(acts[0], dn[0, :, at]) + dot(acts[1], dn[1, :, at])
            ).astype(BF16)
        t_send[k] = dot(pout[...], ybuf[...]).astype(BF16)

        @pl.loop(1, NSP)
        def _(i):
            to = lax.rem(sp + i, NSP)
            pltpu.make_async_remote_copy(
                src_ref=t_send.at[k, slot_rows(to)], dst_ref=t_recv.at[k, slot_rows(sp)],
                send_sem=t_ss.at[k], recv_sem=t_rs.at[k],
                device_id={"sp": to, "tp": tp}, device_id_type=MESH,
            ).start()

        t_recv[k, slot_rows(sp)] = t_send[k, slot_rows(sp)]

    def combined(k):
        pltpu.make_async_copy(t_recv.at[k, others], t_recv.at[k, others], t_rs.at[k]).wait()
        tab = tab_ref[block_of(k)]
        place = iota((TROWS, ROWS), 1).astype(F32)
        weight = jnp.where(place == tab[:, 0:1], tab[:, 2:3], 0.0) + jnp.where(
            place == tab[:, 1:2], tab[:, 3:4], 0.0
        )
        w_h, w_l = two_parts(weight)
        rows = t_recv[k]
        return dot(w_h, rows) + dot(w_l, rows)

    def combine(k):
        mixed = combined(k)

        @pl.when(k == 0)
        def _():
            own[...] = mixed

        @pl.when(k == 1)
        def _():
            r2_send[k] = mixed.astype(BF16)
            total_copy(k).start()

        @pl.when(k > 1)
        def _():
            total_copy(k - 1).wait_recv()
            r2_send[k] = (mixed + r2_recv[k].astype(F32)).astype(BF16)
            total_copy(k).start()

    @pl.loop(0, NZ)
    def _(k):
        @pl.loop(0, PIECES)
        def _(p):
            @pl.when(k > 0)
            def _():
                row_copy(k - 1, p).wait_recv()

            @pl.when(k < NZ - 1)
            def _():
                row_copy(k, p).start()

        experts(k)

        @pl.when(k > 0)
        def _():
            combine(k - 1)

    combine(NZ - 1)
    total_copy(NZ - 1).wait_recv()
    result = (am[...].astype(F32) + (own[...] + r2_recv[NZ].astype(F32))).astype(BF16).astype(F32)
    for j in range(GROUPS):
        out_ref[:, j * WIDE : (j + 1) * WIDE] = result[j * TOK : (j + 1) * TOK].astype(BF16)

    @pl.loop(1, NZ)
    def _(k):
        total_copy(k).wait_send()

        @pl.loop(0, PIECES)
        def _(p):
            sum_copy(k, p).wait_send()
            row_copy(k - 1, p).wait_send()

    @pl.loop(0, NZ)
    def _(k):
        pltpu.make_async_copy(t_send.at[k, others], t_send.at[k, others], t_ss.at[k]).wait()


def grouped(x):
    rows = x.shape[0]
    return x.reshape(rows, GROUPS, WIDE).transpose(1, 0, 2).reshape(GROUPS * rows, WIDE)


def local(
    queries,
    cell_key_rows,
    cell_value_rows,
    output_gate_logits,
    input_gate_logs,
    forget_gate_logits,
    extra_log_forget,
    head_norm_gain,
    cell_output_matrix,
    residual,
    expert_norm_gain,
    routes,
    token_expert_weights,
    expert_gate_matrix,
    expert_up_matrix,
    expert_down_matrix,
):
    tp = lax.axis_index("tp")
    core, z = tp % 2, tp // 2
    resid = grouped(lax.dynamic_slice_in_dim(residual, tp * TOK, TOK, 0))

    def of_core(array):
        return lax.dynamic_index_in_dim(
            array.reshape(NZ, 2, TOK, 2), core, axis=1, keepdims=False
        )

    named = of_core(routes)
    weights = of_core(token_expert_weights)
    onehot = (named[..., None] == jnp.arange(NSP, dtype=jnp.int32)).astype(F32)
    earlier = jnp.tril(jnp.ones((TOK, TOK), F32), -1)
    ahead = jnp.einsum("ij,zje->zie", earlier, jnp.sum(onehot, axis=2))
    position = jnp.sum(ahead[:, :, None, :] * onehot, axis=3)
    base = named.astype(F32) * SLOT + position
    shift = CAP * jnp.arange(GROUPS, dtype=F32)
    places = base[:, None] + shift[None, :, None, None]
    table = jnp.concatenate(
        [places, jnp.broadcast_to(weights[:, None], places.shape)], axis=3
    ).reshape(NZ, TROWS, 4)
    row_table = lax.dynamic_index_in_dim(table, z, axis=0, keepdims=False)[:, :2].T
    row_table = jnp.pad(row_table, ((0, 6), (0, 0)), constant_values=-1.0)

    n = jnp.arange(ROWS, dtype=jnp.int32)
    per = ROWS // GROUPS
    inward = (n % per) // CAP * SLOT + n // per * CAP + n % CAP
    outward = (n % SLOT) // CAP * per + n // SLOT * CAP + n % CAP
    perms = jnp.stack([inward, outward], axis=1)

    vmem = pl.BlockSpec(memory_space=pltpu.VMEM)
    hbm = pl.BlockSpec(memory_space=pltpu.HBM)
    dma = pltpu.SemaphoreType.DMA
    width = GROUPS * WIDE
    return pl.pallas_call(
        kernel,
        name="layer",
        out_shape=jax.ShapeDtypeStruct((TOK, width), BF16),
        in_specs=[vmem] * 13 + [hbm] * 4,
        out_specs=vmem,
        scratch_shapes=[
            pltpu.VMEM((2, HEAD_DIM, width), BF16),
            pltpu.VMEM((4, width, HEAD_DIM), BF16),
            pltpu.VMEM((2, HEAD_DIM, width), BF16),
            pltpu.VMEM((HEAD_DIM + 8, HEAD_DIM), F32),
            pltpu.VMEM((NSP, HEAD_DIM + 8, HEAD_DIM), F32),
            pltpu.VMEM((NSP, 8, HEAD_DIM), F32),
            pltpu.VMEM((LEN, HEAD_DIM), F32),
            pltpu.VMEM((LEN, HEAD_DIM), F32),
            pltpu.VMEM((LEN // 2, HEAD_DIM), F32),
            pltpu.VMEM((LEN // 2, HEAD_DIM), F32),
            pltpu.VMEM((LEN // 2, HEAD_DIM), BF16),
            pltpu.VMEM((LEN // 2, HEAD_DIM), BF16),
            pltpu.VMEM((NZ, TROWS, WIDE), F32),
            pltpu.VMEM((NZ, TROWS, WIDE), BF16),
            pltpu.VMEM((NZ + 1, TROWS, WIDE), BF16),
            pltpu.VMEM((TROWS, WIDE), BF16),
            pltpu.VMEM((TROWS, WIDE), BF16),
            pltpu.VMEM((ROWS, WIDE), BF16),
            pltpu.VMEM((ROWS, WIDE), BF16),
            pltpu.VMEM((ROWS, ROWS), BF16),
            pltpu.VMEM((ROWS, ROWS), BF16),
            pltpu.VMEM((NZ, ROWS, WIDE), BF16),
            pltpu.VMEM((ROWS, WIDE), BF16),
            pltpu.VMEM((NZ, ROWS, WIDE), BF16),
            pltpu.VMEM((NZ, ROWS, WIDE), BF16),
            pltpu.VMEM((NZ, TROWS, WIDE), BF16),
            pltpu.VMEM((NZ + 1, TROWS, WIDE), BF16),
            pltpu.VMEM((TROWS, WIDE), F32),
            dma((4,)), dma((4,)), dma((4,)), dma((NSP,)), dma((NSP,)), dma((2,)),
            dma((NZ, PIECES)), dma((NZ + 1, PIECES)),
            dma((2,)), dma((NZ - 1, PIECES)), dma((NZ - 1, PIECES)),
            dma((NZ,)), dma((NZ,)), dma((NZ,)), dma((NZ + 1,)),
        ],
        compiler_params=pltpu.CompilerParams(
            collective_id=0, has_side_effects=True, vmem_limit_bytes=60 << 20
        ),
    )(
        queries,
        cell_key_rows,
        cell_value_rows,
        output_gate_logits,
        input_gate_logs,
        forget_gate_logits,
        extra_log_forget,
        head_norm_gain.reshape(1, HEAD_DIM),
        resid,
        expert_norm_gain.reshape(GROUPS, WIDE),
        table,
        row_table,
        perms,
        cell_output_matrix,
        expert_gate_matrix[0],
        expert_up_matrix[0],
        expert_down_matrix[0],
    )


def solution(mesh):
    in_specs = (
        P("sp", "tp"),
        P("sp", "tp"),
        P("sp", "tp"),
        P("sp", "tp"),
        P("tp", "sp"),
        P("tp", "sp"),
        P("tp", "sp"),
        P("tp"),
        P("tp", None),
        P("sp", None),
        P(),
        P("sp", None),
        P("sp", None),
        P("sp", None, "tp"),
        P("sp", None, "tp"),
        P("sp", "tp", None),
    )
    return jax.shard_map(
        local, mesh=mesh, in_specs=in_specs, out_specs=P(("sp", "tp"), None), check_vma=False
    )
```

time: 363 us -> 163 us (0.45)
  waiting for transfers between devices: 229 us -> 0 us
  Pallas kernels: 0 us -> 152 us
  matrix products: 32.4 us -> 0.19 us
  other arithmetic: 25.2 us -> 0.2 us
  blocking collectives: 19.8 us -> 0 us
  between operations: 17.3 us -> 0.15 us
  starting transfers between devices: 14.2 us -> 0 us
  local copies, waits for them, and re-layouts: 20 us -> 8.56 us
  loops' own time: 4.26 us -> 0 us
    pallas_call x0 -> x1, Pallas kernels: none -> 152 us  [local(): pl.pallas_call(kernel, name='layer', out_shape=jax.ShapeDtypeStruct((TOK,...]
    reduce_scatter x3 -> x0, waiting for transfers between devices: 139 us -> none  [the longest x1 77.4 us: local(): lax.psum_scatter(jnp.einsum('rcf,fd->rcd', hidden, down_local, preferred_...]
    all_gather x1 -> x0, waiting for transfers between devices: 69.9 us -> none  [local(): piece = lax.all_gather(arrived, TP, axis=0, tiled=True)]
    dot_general x17 -> x1, matrix products: 32.4 us -> 0.19 us  [local(): ahead = jnp.einsum('ij,zje->zie', earlier, jnp.sum(onehot, axis=2))]
    all_to_all x1 -> x0, blocking collectives: 19.8 us -> none  [local(): lax.all_to_all(sent, 'sp', split_axis=0, concat_axis=0, tiled=True)]
    all_to_all x2 -> x0, waiting for transfers between devices: 19.8 us -> none  [the longest x1 19.8 us: local(): lax.all_to_all(summed, 'sp', split_axis=0, concat_axis=0, tiled=True)]
    all_to_all x2 -> x0, starting transfers between devices: 13.8 us -> none  [the longest x1 7.03 us: from_everyone(): lax.all_to_all(jnp.broadcast_to(x[None], (count, *x.shape)), axis, 0, 0,...]
    reduce_max x7 -> x0, other arithmetic: 8.55 us -> none  [the longest x3 6.01 us: advance(): stab_next = jnp.maximum(total + stab, jnp.max(log_write, axis=-1))]
  transfers between devices with their start and end apart: 6 -> 0, of which waited for: 5 -> 0; matrix products, arithmetic and copies ran while one was open for 6% -> 0% of each run, Pallas kernels for 0% -> 0%
where the time goes in v1:
time: 163 us; the launch traced here: 162 us
  Pallas kernels  152 us (93%)
  local copies, waits for them, and re-layouts  8.56 us (5%)
    pallas_call x1, Pallas kernels, local(): pl.pallas_call(kernel, name='layer', out_shape=jax.ShapeDtypeStruct((TOK,...  152 us

profile of v1, /device:TPU:32, one launch (start us, length us, event | category | flops | bytes accessed | tf_op | source)
XLA Modules:
  0.0 161.5 jit_solution(18396334830049106816)
XLA Ops:
  0.0 0.0 copy-start
  0.0 0.1 add.179
  0.1 0.1 add.180
  0.2 0.1 fusion.9
  0.3 1.5 reshape.210.eng_ref
  1.7 0.8 reshape.211
  2.6 0.8 reshape.212
  3.4 0.2 convolution_bitcast_fusion
  3.7 0.1 add.178
  3.8 0.1 concatenate.6
  3.9 0.6 pad.4.rowtab_ref
  4.5 0.0 copy-done
  4.5 0.1 copy.47
  4.6 0.7 copy.37
  5.3 0.9 copy.43.perm_ref
  6.3 1.2 copy.42.tab_ref
  7.5 152.4 %layer.1 = bf16[24,4096]{1,0:T(8,128)(2,1)} custom-call(bf16[384,128]{1,0:T(8,128)(2,1)} %q_ref.1, bf16[384,128]{1,0:T(8,128)(2,1)} %k_ref.1, bf16[384,128]{1,0:T(8,128)(2,1)} %v_ref.1, bf16[384,128]{1,0:T(8,128)(2,1)} %og_ref.1, f32[1,384]{1,0:T(1,128)} %ig_ref.1, f32[1,384]{1,0:T(1,128)} %fg_ref.1, f32[1,384]{1,0:T(1,128)} %ex_ref.1, f32[1,128]{1,0:T(1,128)} %bitcast.52, ...), custom_call_target="tpu_custom_call" | custom-call | tf_op jit(solution)/shard_map/layer/pallas_call | solution.py:464
  159.9 1.6 %copy.54 = bf16[24,4096]{1,0:T(8,128)(2,1)} copy(bf16[24,4096]{1,0:T(8,128)(2,1)} %layer.1) | data formatting | bytes 393216
  (18 shorter events, 0.2 us)
Async XLA Ops:
  0.0 4.5 %copy-start = (bf16[384,4096]{1,0:T(8,128)(2,1)S(1)}, bf16[384,4096]{1,0:T(8,128)(2,1)}, u32[]{:S(2)}) copy-start(bf16[384,4096]{1,0:T(8,128)(2,1)} %param.25) | copy-start | bytes 9437188

commit v2 on v1

v2 whole, which is shorter than its diff:
```python
import jax
import jax.numpy as jnp
from jax import lax
from jax.experimental import pallas as pl
from jax.experimental.pallas import tpu as pltpu
from jax.sharding import PartitionSpec as P

MESH = pl.DeviceIdType.MESH
F32 = jnp.float32
BF16 = jnp.bfloat16

HEAD_DIM = 128
NSP = 16
NZ = 8
LEN = 384
TOK = 24
CAP = 6
GROUPS = 16
WIDE = 256
TURNS = 2
GT = GROUPS // TURNS
SLOT = GT * CAP
ROWS = NSP * SLOT
TROWS = GROUPS * TOK
HROWS = GT * TOK
PER = ROWS // GT
NX = 4
PIECES = 2
STRIPES = 4

floor_neg = -1e30
norm_eps = 1e-06


def dot(a, b):
    return jnp.dot(a, b, preferred_element_type=F32)


def two_parts(x):
    high = x.astype(BF16)
    return high, (x - high.astype(F32)).astype(BF16)


def iota(shape, dim):
    return lax.broadcasted_iota(jnp.int32, shape, dim)


def kernel(
    q_ref, k_ref, v_ref, og_ref, ig_ref, fg_ref, ex_ref, hg_ref,
    eng_ref, route_ref, weight_ref,
    resid_hbm, wo_hbm, gate_hbm, up_hbm, down_hbm,
    out_ref,
    wv, gw, dn, resid,
    row_s, tot_send, tot_s, gs, num_s, co_f, co_a, co_b, co_send, co_recv,
    pf, r1_send, r1_recv, am,
    d_send, d_recv, pin, pout, pick, table,
    xring, acc_s, sq_s, ybuf, mixer, t_send, t_recv, r2_send, r2_recv, own,
    load_sem, wx_send, wx_recv, row_ss, row_rs, tot_ss, tot_rs, co_sem, r1_ss, r1_rs,
    d_ss, d_rs, x_ss, x_rs, t_ss, t_rs, r2_ss, r2_rs,
):
    sp = lax.axis_index("sp")
    tp = lax.axis_index("tp")
    core = lax.rem(tp, 2)
    z = tp // 2
    step = jnp.where(core == 0, 1, NZ - 1)
    above = lax.rem(z + 1, NZ) * 2 + core
    below = lax.rem(z + NZ - 1, NZ) * 2 + core
    after = jnp.where(core == 0, above, below)
    mate = z * 2 + 1 - core
    y, x = sp // NX, lax.rem(sp, NX)

    barrier = pltpu.get_barrier_semaphore()

    @pl.loop(1, NSP)
    def _(i):
        pl.semaphore_signal(
            barrier, inc=1, device_id={"sp": lax.rem(sp + i, NSP), "tp": tp}, device_id_type=MESH
        )

    for other in (above, below, mate):
        pl.semaphore_signal(barrier, inc=1, device_id={"sp": sp, "tp": other}, device_id_type=MESH)

    loads = [
        pltpu.make_async_copy(wo_hbm, wv.at[0], load_sem.at[0]),
        pltpu.make_async_copy(gate_hbm, gw.at[0], load_sem.at[1]),
        pltpu.make_async_copy(up_hbm, gw.at[1], load_sem.at[2]),
        pltpu.make_async_copy(down_hbm, dn.at[0], load_sem.at[3]),
        pltpu.make_async_copy(
            resid_hbm.at[pl.ds(pl.multiple_of(tp * TOK, 8), TOK)], resid, load_sem.at[4]
        ),
    ]
    for load in loads:
        load.start()

    tt = iota((LEN, LEN), 0)
    ss = iota((LEN, LEN), 1)
    causal = ss <= tt
    fg = fg_ref[...]
    f_row = jnp.minimum(fg, 0.0) - jnp.log1p(jnp.exp(-jnp.abs(fg))) + ex_ref[...]
    i_row = ig_ref[...]
    f_all = jnp.broadcast_to(f_row, (LEN, LEN))
    f_col = jnp.sum(jnp.where(ss == tt, f_all, 0.0), axis=1, keepdims=True)
    i_col = jnp.sum(
        jnp.where(ss == tt, jnp.broadcast_to(i_row, (LEN, LEN)), 0.0), axis=1, keepdims=True
    )
    c_col = jnp.sum(jnp.where(causal, f_all, 0.0), axis=1, keepdims=True)
    c_row = jnp.sum(
        jnp.where(tt <= ss, jnp.broadcast_to(f_col, (LEN, LEN)), 0.0), axis=0, keepdims=True
    )
    total = jnp.sum(f_row, axis=1, keepdims=True)
    scale = HEAD_DIM ** (-0.5)
    write = i_col + total - c_col
    stab_dev = jnp.max(write, axis=0, keepdims=True)
    kw = k_ref[...].astype(F32) * (jnp.exp(write - stab_dev) * scale)
    kw_h, kw_l = two_parts(kw)
    dims = (((0,), (0,)), ((), ()))
    v = v_ref[...]
    cell_dev = lax.dot_general(kw_h, v, dims, preferred_element_type=F32) + lax.dot_general(
        kw_l, v, dims, preferred_element_type=F32
    )

    def packed(cell, stab, tot):
        numbers = jnp.where(
            iota((8, HEAD_DIM), 0) == 0,
            jnp.broadcast_to(stab, (8, HEAD_DIM)),
            jnp.broadcast_to(tot, (8, HEAD_DIM)),
        )
        return jnp.concatenate([cell, numbers], axis=0)

    row_s[x] = packed(cell_dev, stab_dev, total)
    q = q_ref[...]
    scores = lax.dot_general(
        q, k_ref[...], (((1,), (1,)), ((), ())), preferred_element_type=F32
    ) * scale
    inner = jnp.where(causal, c_col - c_row + i_row, floor_neg)
    top = jnp.max(inner, axis=1, keepdims=True)
    p_h, p_l = two_parts(scores * jnp.exp(inner - top))
    num_s[...] = dot(p_h, v) + dot(p_l, v)

    def part_of(n, size):
        return jnp.floor((n.astype(F32) + 0.5) * (1.0 / size))

    same = part_of(iota((LEN, 1), 0), TOK) == part_of(iota((1, LEN), 1), TOK)
    earlier = jnp.where(same & (tt < ss), 1.0, 0.0).astype(BF16)
    named = [iota((NSP, LEN), 0) == route_ref[i : i + 1, :] for i in range(2)]
    onehot = [jnp.where(n, 1.0, 0.0) for n in named]
    ahead = dot((onehot[0] + onehot[1]).astype(BF16), earlier)
    places = [jnp.sum(ahead * o, axis=0, keepdims=True) for o in onehot]
    line = iota((HEAD_DIM, LEN), 0)
    rows = jnp.zeros((HEAD_DIM, LEN), F32)
    for i in range(2):
        rows = jnp.where(line == i, route_ref[i : i + 1, :].astype(F32) * SLOT + places[i], rows)
        rows = jnp.where(line == i + 2, weight_ref[i : i + 1, :], rows)
    table[...] = jnp.transpose(rows)

    def spots(tokens):
        return [
            jnp.concatenate([tokens[:, i : i + 1] + CAP * j for j in range(GT)], axis=0)
            for i in range(2)
        ]

    def block_rows(block):
        return pl.ds(pl.multiple_of(block * TOK, 8), TOK)

    place = iota((HROWS, ROWS), 1).astype(F32)
    first, second = spots(table[block_rows(tp), :])
    pick[...] = jnp.transpose(
        jnp.where((place == first) | (place == second), 1.0, 0.0)
    ).astype(BF16)

    def reordered(outer, middle):
        n = iota((ROWS, 1), 0)
        a = part_of(n, outer)
        rest = n.astype(F32) - outer * a
        b = jnp.floor((rest + 0.5) * (1.0 / CAP))
        source = b * middle + a * CAP + (rest - CAP * b)
        return jnp.where(iota((ROWS, ROWS), 1).astype(F32) == source, 1.0, 0.0).astype(BF16)

    pin[...] = reordered(PER, SLOT)
    pout[...] = reordered(SLOT, PER)

    pl.semaphore_wait(barrier, NSP - 1 + 3)

    def row_copy_x(i):
        return pltpu.make_async_remote_copy(
            src_ref=row_s.at[x], dst_ref=row_s.at[x], send_sem=row_ss.at[i], recv_sem=row_rs.at[x],
            device_id={"sp": y * NX + lax.rem(x + i, NX), "tp": tp}, device_id_type=MESH,
        )

    def row_arrival(source):
        return pltpu.make_async_remote_copy(
            src_ref=row_s.at[source], dst_ref=row_s.at[source],
            send_sem=row_ss.at[0], recv_sem=row_rs.at[source],
            device_id={"sp": sp, "tp": mate}, device_id_type=MESH,
        )

    def total_row_copy(to, source):
        return pltpu.make_async_remote_copy(
            src_ref=tot_send, dst_ref=tot_s.at[source],
            send_sem=tot_ss.at[to], recv_sem=tot_rs.at[source],
            device_id={"sp": to * NX + x, "tp": tp}, device_id_type=MESH,
        )

    for i in range(1, NX):
        row_copy_x(i).start()

    pairs = [(wo_hbm, wv.at[1]), (gate_hbm, gw.at[2]), (up_hbm, gw.at[3]), (down_hbm, dn.at[1])]
    shared = [
        pltpu.make_async_remote_copy(
            src_ref=source, dst_ref=target, send_sem=wx_send.at[i], recv_sem=wx_recv.at[i],
            device_id={"sp": sp, "tp": mate}, device_id_type=MESH,
        )
        for i, (source, target) in enumerate(pairs)
    ]
    for copy in shared:
        copy.start()

    for i in range(1, NX):
        row_arrival(lax.rem(x + i, NX)).wait_recv()

    low = jnp.full((1, HEAD_DIM), floor_neg, F32)
    none = jnp.zeros((1, HEAD_DIM), F32)
    blank = jnp.zeros((HEAD_DIM, HEAD_DIM), F32)

    def fold(buffer, at, count, carry):
        def one(i, carry):
            top, tot = carry
            n = count - 1 - i
            here = buffer[n, HEAD_DIM : HEAD_DIM + 1, :] + tot
            gs[at + n, 0:1, :] = here
            return jnp.maximum(top, here), tot + buffer[n, HEAD_DIM + 1 : HEAD_DIM + 2, :]

        return lax.fori_loop(0, count, one, carry)

    def weighted(buffer, at, count, stab, cell):
        def one(n, cell):
            return cell + jnp.exp(gs[at + n, 0:1, :] - stab) * buffer[n, :HEAD_DIM, :]

        return lax.fori_loop(0, count, one, cell)

    row_stab, row_tot = fold(row_s, 0, NX, (low, none))
    tot_send[...] = packed(weighted(row_s, 0, NX, row_stab, blank), row_stab, row_tot)

    @pl.loop(y + 1, NX)
    def _(to):
        total_row_copy(to, y).start()

    carry = fold(row_s, 0, x, (low, none))

    @pl.loop(0, y)
    def _(source):
        total_row_copy(source, source).wait_recv()

    stab0, tot0 = fold(tot_s, NX, y, carry)
    start_stab = jnp.maximum(stab0, tot0)
    start_cell = weighted(row_s, 0, x, start_stab, blank)
    cell_h, cell_l = two_parts(weighted(tot_s, NX, y, start_stab, start_cell))
    carried = c_col + start_stab[:, 0:1]
    stab = jnp.maximum(top, carried)
    numer = jnp.exp(top - stab) * num_s[...] + jnp.exp(carried - stab) * (
        dot(q, cell_h) + dot(q, cell_l)
    )
    scaled = (
        numer
        * lax.rsqrt(jnp.mean(numer * numer, axis=1, keepdims=True) + norm_eps)
        * hg_ref[...]
    )
    co_f[...] = scaled / (1.0 + jnp.exp(-og_ref[...].astype(F32)))
    for i in range(NZ):
        mine = pl.multiple_of((2 * i + core) * TOK, 8)
        theirs = pl.multiple_of((2 * i + 1 - core) * TOK, 8)
        co_a[i * TOK : (i + 1) * TOK, :] = co_f[pl.ds(mine, TOK), :]
        co_b[i * TOK : (i + 1) * TOK, :] = co_f[pl.ds(theirs, TOK), :]
    co_send[...] = co_b[...].astype(BF16)
    swap = pltpu.make_async_remote_copy(
        src_ref=co_send, dst_ref=co_recv, send_sem=co_sem.at[0], recv_sem=co_sem.at[1],
        device_id={"sp": sp, "tp": mate}, device_id_type=MESH,
    )
    swap.start()
    mine_b = co_a[...].astype(BF16)

    for i in range(1, NX):
        row_copy_x(i).wait_send()

    @pl.loop(y + 1, NX)
    def _(to):
        total_row_copy(to, y).wait_send()

    loads[0].wait()
    shared[0].wait()
    swap.wait()
    both = jnp.concatenate([mine_b, co_recv[...]], axis=1)

    @pl.loop(0, GROUPS)
    def _(j):
        at = pl.ds(pl.multiple_of(j * WIDE, WIDE), WIDE)
        part = dot(both, wv[:, :, at].reshape(2 * HEAD_DIM, WIDE))
        for i in range(NZ):
            pf[i, pl.ds(pl.multiple_of(j * TOK, 8), TOK), :] = part[i * TOK : (i + 1) * TOK]

    srows = TROWS // STRIPES

    def hops(d, p):
        return 4 if (p % 2 == 0) == (d == 0) else 3

    def sum_copy(d, m, p):
        rows = pl.ds(p * srows, srows)
        return pltpu.make_async_remote_copy(
            src_ref=r1_send.at[d, m, rows], dst_ref=r1_recv.at[d, m, rows],
            send_sem=r1_ss.at[d, m, p], recv_sem=r1_rs.at[d, m, p],
            device_id={"sp": sp, "tp": (above, below)[d]}, device_id_type=MESH,
        )

    def sum_steps(h, m):
        for d in range(2):
            for p in sorted((2 * h, 2 * h + 1), key=lambda p: -hops(d, p)):
                left = hops(d, p) - m
                if left > 0:
                    rows = slice(p * srows, (p + 1) * srows)
                    part = pf[lax.rem(z + (left if d == 0 else NZ - left), NZ), rows]
                    if m > 0:
                        sum_copy(d, m - 1, p).wait_recv()
                        part = part + r1_recv[d, m - 1, rows].astype(F32)
                    r1_send[d, m, rows] = part.astype(BF16)
                    sum_copy(d, m, p).start()

    def slot_rows(s):
        return pl.ds(pl.multiple_of(s * SLOT, SLOT), SLOT)

    def dispatch(h):
        for p in (2 * h, 2 * h + 1):
            rows = slice(p * srows, (p + 1) * srows)
            for d in range(2):
                sum_copy(d, hops(d, p) - 1, p).wait_recv()
            sides = [r1_recv[d, hops(d, p) - 1, rows].astype(F32) for d in range(2)]
            width = srows // TOK
            old = jnp.concatenate(
                [
                    resid[:, j * WIDE : (j + 1) * WIDE].astype(F32)
                    for j in range(p * width, (p + 1) * width)
                ],
                axis=0,
            )
            am[rows] = (old + (pf[z, rows] + sides[0] + sides[1])).astype(BF16)
        d_send[h] = dot(pick[...], am[h * HROWS : (h + 1) * HROWS]).astype(BF16)

        @pl.loop(1, NSP)
        def _(i):
            to = lax.rem(sp + i, NSP)
            pltpu.make_async_remote_copy(
                src_ref=d_send.at[h, slot_rows(to)], dst_ref=d_recv.at[h, slot_rows(sp)],
                send_sem=d_ss.at[h], recv_sem=d_rs.at[h],
                device_id={"sp": to, "tp": tp}, device_id_type=MESH,
            ).start()

        d_recv[h, slot_rows(sp)] = d_send[h, slot_rows(sp)]

    loads[4].wait()
    sum_steps(0, 0)
    for m in range(1, 4):
        sum_steps(0, m)
        sum_steps(1, m - 1)
    dispatch(0)
    sum_steps(1, 3)
    dispatch(1)

    for load in loads[1:4]:
        load.wait()
    for copy in shared[1:]:
        copy.wait()

    others = pl.ds(0, ROWS - SLOT)
    xrows = ROWS // PIECES

    def block_of(k):
        return lax.rem(z + NZ * NZ - step * k, NZ)

    def row_copy(k, h, p):
        rows = pl.ds(pl.multiple_of(p * xrows, xrows), xrows)
        return pltpu.make_async_remote_copy(
            src_ref=xring.at[k, h, rows], dst_ref=xring.at[k + 1, h, rows],
            send_sem=x_ss.at[k, h, p], recv_sem=x_rs.at[k, h, p],
            device_id={"sp": sp, "tp": after}, device_id_type=MESH,
        )

    def total_copy(k, h):
        return pltpu.make_async_remote_copy(
            src_ref=r2_send.at[k, h], dst_ref=r2_recv.at[k + 1, h],
            send_sem=r2_ss.at[k, h], recv_sem=r2_rs.at[k + 1, h],
            device_id={"sp": sp, "tp": after}, device_id_type=MESH,
        )

    def arrive(k, h):
        @pl.when(k == 0)
        def _():
            pltpu.make_async_copy(d_recv.at[h, others], d_recv.at[h, others], d_rs.at[h]).wait()
            xring[0, h] = dot(pin[...], d_recv[h]).astype(BF16)

        @pl.loop(0, PIECES)
        def _(p):
            @pl.when(k > 0)
            def _():
                row_copy(k - 1, h, p).wait_recv()

            @pl.when(k < NZ - 1)
            def _():
                row_copy(k, h, p).start()

    def first_part(k, h):
        acc = jnp.zeros((PER, 4 * HEAD_DIM), F32)
        squares = jnp.zeros((PER, WIDE), F32)
        for j in range(GT):
            at = slice((h * GT + j) * WIDE, (h * GT + j + 1) * WIDE)
            rows = xring[k, h, j * PER : (j + 1) * PER, :].astype(F32)
            squares = squares + rows * rows
            w = jnp.concatenate([gw[i, at, :] for i in range(4)], axis=1)
            acc = acc + dot((rows * eng_ref[:, at]).astype(BF16), w)
        return acc, squares

    def second_part(k, acc, squares):
        mean = jnp.sum(squares, axis=1, keepdims=True) * (1.0 / (GROUPS * WIDE))
        acc = acc * lax.rsqrt(mean + norm_eps)
        acts = []
        for i in range(2):
            gate = acc[:, 2 * i * HEAD_DIM : (2 * i + 1) * HEAD_DIM]
            upper = acc[:, (2 * i + 1) * HEAD_DIM : (2 * i + 2) * HEAD_DIM]
            acts.append((gate / (1.0 + jnp.exp(-gate)) * upper).astype(BF16))
        act = jnp.concatenate(acts, axis=1)
        for h in range(TURNS):
            for j in range(GT):
                at = slice((h * GT + j) * WIDE, (h * GT + j + 1) * WIDE)
                w = dn[:, :, at].reshape(2 * HEAD_DIM, WIDE)
                ybuf[h, j * PER : (j + 1) * PER, :] = dot(act, w).astype(BF16)
            t_send[k, h] = dot(pout[...], ybuf[h]).astype(BF16)

            @pl.loop(1, NSP)
            def _(i, h=h):
                to = lax.rem(sp + i, NSP)
                pltpu.make_async_remote_copy(
                    src_ref=t_send.at[k, h, slot_rows(to)], dst_ref=t_recv.at[k, h, slot_rows(sp)],
                    send_sem=t_ss.at[k, h], recv_sem=t_rs.at[k, h],
                    device_id={"sp": to, "tp": tp}, device_id_type=MESH,
                ).start()

            t_recv[k, h, slot_rows(sp)] = t_send[k, h, slot_rows(sp)]

    def combine(k, h):
        if h == 0:
            tokens = table[block_rows(block_of(k) * 2 + core), :]
            first, second = spots(tokens)
            weights = [jnp.concatenate([tokens[:, i : i + 1]] * GT, axis=0) for i in (2, 3)]
            place = iota((HROWS, ROWS), 1).astype(F32)
            weight = jnp.where(place == first, weights[0], 0.0) + jnp.where(
                place == second, weights[1], 0.0
            )
            w_h, w_l = two_parts(weight)
            mixer[:HROWS] = w_h
            mixer[HROWS:] = w_l
        pltpu.make_async_copy(
            t_recv.at[k, h, others], t_recv.at[k, h, others], t_rs.at[k, h]
        ).wait()
        mixed = dot(mixer[...], t_recv[k, h])
        mixed = mixed[:HROWS] + mixed[HROWS:]

        @pl.when(k == 0)
        def _():
            own[h] = mixed

        @pl.when(k == 1)
        def _():
            r2_send[k, h] = mixed.astype(BF16)
            total_copy(k, h).start()

        @pl.when(k > 1)
        def _():
            total_copy(k - 1, h).wait_recv()
            r2_send[k, h] = (mixed + r2_recv[k, h].astype(F32)).astype(BF16)
            total_copy(k, h).start()

    @pl.loop(0, NZ)
    def _(k):
        arrive(k, 0)
        acc, squares = first_part(k, 0)
        acc_s[...] = acc
        sq_s[...] = squares

        @pl.when(k > 0)
        def _():
            combine(k - 1, 0)

        arrive(k, 1)
        acc, squares = first_part(k, 1)
        second_part(k, acc_s[...] + acc, sq_s[...] + squares)

        @pl.when(k > 0)
        def _():
            combine(k - 1, 1)

    for h in range(TURNS):
        combine(NZ - 1, h)
    for h in range(TURNS):
        total_copy(NZ - 1, h).wait_recv()
        result = am[h * HROWS : (h + 1) * HROWS].astype(F32) + (
            own[h] + r2_recv[NZ, h].astype(F32)
        )
        for j in range(GT):
            at = slice((h * GT + j) * WIDE, (h * GT + j + 1) * WIDE)
            out_ref[:, at] = result[j * TOK : (j + 1) * TOK].astype(BF16)

    for d in range(2):
        for p in range(STRIPES):
            for m in range(hops(d, p)):
                sum_copy(d, m, p).wait_send()

    @pl.loop(1, NZ)
    def _(k):
        @pl.loop(0, TURNS)
        def _(h):
            total_copy(k, h).wait_send()

            @pl.loop(0, PIECES)
            def _(p):
                row_copy(k - 1, h, p).wait_send()

    @pl.loop(0, TURNS)
    def _(h):
        pltpu.make_async_copy(d_send.at[h, others], d_send.at[h, others], d_ss.at[h]).wait()

        @pl.loop(0, NZ)
        def _(k):
            pltpu.make_async_copy(
                t_send.at[k, h, others], t_send.at[k, h, others], t_ss.at[k, h]
            ).wait()


def local(
    queries,
    cell_key_rows,
    cell_value_rows,
    output_gate_logits,
    input_gate_logs,
    forget_gate_logits,
    extra_log_forget,
    head_norm_gain,
    cell_output_matrix,
    residual,
    expert_norm_gain,
    routes,
    token_expert_weights,
    expert_gate_matrix,
    expert_up_matrix,
    expert_down_matrix,
):
    vmem = pl.BlockSpec(memory_space=pltpu.VMEM)
    hbm = pl.BlockSpec(memory_space=pltpu.HBM)
    dma = pltpu.SemaphoreType.DMA
    width = GROUPS * WIDE
    return pl.pallas_call(
        kernel,
        name="layer",
        out_shape=jax.ShapeDtypeStruct((TOK, width), BF16),
        in_specs=[vmem] * 11 + [hbm] * 5,
        out_specs=vmem,
        scratch_shapes=[
            pltpu.VMEM((2, HEAD_DIM, width), BF16),
            pltpu.VMEM((4, width, HEAD_DIM), BF16),
            pltpu.VMEM((2, HEAD_DIM, width), BF16),
            pltpu.VMEM((TOK, width), BF16),
            pltpu.VMEM((NX, HEAD_DIM + 8, HEAD_DIM), F32),
            pltpu.VMEM((HEAD_DIM + 8, HEAD_DIM), F32),
            pltpu.VMEM((NX, HEAD_DIM + 8, HEAD_DIM), F32),
            pltpu.VMEM((NSP, 8, HEAD_DIM), F32),
            pltpu.VMEM((LEN, HEAD_DIM), F32),
            pltpu.VMEM((LEN, HEAD_DIM), F32),
            pltpu.VMEM((LEN // 2, HEAD_DIM), F32),
            pltpu.VMEM((LEN // 2, HEAD_DIM), F32),
            pltpu.VMEM((LEN // 2, HEAD_DIM), BF16),
            pltpu.VMEM((LEN // 2, HEAD_DIM), BF16),
            pltpu.VMEM((NZ, TROWS, WIDE), F32),
            pltpu.VMEM((2, 4, TROWS, WIDE), BF16),
            pltpu.VMEM((2, 4, TROWS, WIDE), BF16),
            pltpu.VMEM((TROWS, WIDE), BF16),
            pltpu.VMEM((TURNS, ROWS, WIDE), BF16),
            pltpu.VMEM((TURNS, ROWS, WIDE), BF16),
            pltpu.VMEM((ROWS, ROWS), BF16),
            pltpu.VMEM((ROWS, ROWS), BF16),
            pltpu.VMEM((ROWS, HROWS), BF16),
            pltpu.VMEM((LEN, HEAD_DIM), F32),
            pltpu.VMEM((NZ, TURNS, ROWS, WIDE), BF16),
            pltpu.VMEM((PER, 4 * HEAD_DIM), F32),
            pltpu.VMEM((PER, WIDE), F32),
            pltpu.VMEM((TURNS, ROWS, WIDE), BF16),
            pltpu.VMEM((2 * HROWS, ROWS), BF16),
            pltpu.VMEM((NZ, TURNS, ROWS, WIDE), BF16),
            pltpu.VMEM((NZ, TURNS, ROWS, WIDE), BF16),
            pltpu.VMEM((NZ, TURNS, HROWS, WIDE), BF16),
            pltpu.VMEM((NZ + 1, TURNS, HROWS, WIDE), BF16),
            pltpu.VMEM((TURNS, HROWS, WIDE), F32),
            dma((5,)), dma((4,)), dma((4,)), dma((NX,)), dma((NX,)), dma((NX,)), dma((NX,)), dma((2,)),
            dma((2, 4, STRIPES)), dma((2, 4, STRIPES)),
            dma((TURNS,)), dma((TURNS,)),
            dma((NZ - 1, TURNS, PIECES)), dma((NZ - 1, TURNS, PIECES)),
            dma((NZ, TURNS)), dma((NZ, TURNS)), dma((NZ, TURNS)), dma((NZ + 1, TURNS)),
        ],
        compiler_params=pltpu.CompilerParams(
            collective_id=0, has_side_effects=True, vmem_limit_bytes=60 << 20
        ),
    )(
        queries,
        cell_key_rows,
        cell_value_rows,
        output_gate_logits,
        input_gate_logs,
        forget_gate_logits,
        extra_log_forget,
        head_norm_gain.reshape(1, HEAD_DIM),
        expert_norm_gain.reshape(1, width),
        routes.T,
        token_expert_weights.T,
        residual,
        cell_output_matrix,
        expert_gate_matrix[0],
        expert_up_matrix[0],
        expert_down_matrix[0],
    )


def solution(mesh):
    in_specs = (
        P("sp", "tp"),
        P("sp", "tp"),
        P("sp", "tp"),
        P("sp", "tp"),
        P("tp", "sp"),
        P("tp", "sp"),
        P("tp", "sp"),
        P("tp"),
        P("tp", None),
        P("sp", None),
        P(),
        P("sp", None),
        P("sp", None),
        P("sp", None, "tp"),
        P("sp", None, "tp"),
        P("sp", "tp", None),
    )
    return jax.shard_map(
        local, mesh=mesh, in_specs=in_specs, out_specs=P(("sp", "tp"), None), check_vma=False
    )
```

time: 163 us -> 139 us (0.85)
  Pallas kernels: 152 us -> 137 us
  local copies, waits for them, and re-layouts: 8.56 us -> 1.62 us
    pallas_call x1, Pallas kernels: 152 us -> 137 us  [local(): pl.pallas_call(kernel, name='layer', out_shape=jax.ShapeDtypeStruct((TOK,...]
    reshape x3 -> x0, local copies, waits for them, and re-layouts: 3.03 us -> none  [the longest x2 1.55 us: of_core(): array.reshape(NZ, 2, TOK, 2)]
where the time goes in v2:
time: 139 us
  Pallas kernels  137 us (99%)
  local copies, waits for them, and re-layouts  1.62 us (1%)
    pallas_call x1, Pallas kernels, local(): pl.pallas_call(kernel, name='layer', out_shape=jax.ShapeDtypeStruct((TOK,...  137 us

profile of v2, /device:TPU:32, one launch (start us, length us, event | category | flops | bytes accessed | tf_op | source)
XLA Modules:
  0.0 139.0 jit_solution(13510748705589981409)
XLA Ops:
  0.0 137.4 %layer.1 = bf16[24,4096]{1,0:T(8,128)(2,1)} custom-call(bf16[384,128]{1,0:T(8,128)(2,1)} %q_ref.1, bf16[384,128]{1,0:T(8,128)(2,1)} %k_ref.1, bf16[384,128]{1,0:T(8,128)(2,1)} %v_ref.1, bf16[384,128]{1,0:T(8,128)(2,1)} %og_ref.1, f32[1,384]{1,0:T(1,128)} %ig_ref.1, f32[1,384]{1,0:T(1,128)} %fg_ref.1, f32[1,384]{1,0:T(1,128)} %ex_ref.1, f32[1,128]{1,0:T(1,128)} %bitcast.13, ...), custom_call_target="tpu_custom_call" | custom-call | tf_op jit(solution)/shard_map/layer/pallas_call | solution.py:558
  137.4 1.6 %copy.18 = bf16[24,4096]{1,0:T(8,128)(2,1)} copy(bf16[24,4096]{1,0:T(8,128)(2,1)} %layer.1) | data formatting | bytes 393216

commit v3 on v2

--- a/solution.py
+++ b/solution.py
@@ -53,10 +53,10 @@
     wv, gw, dn, resid,
     row_s, tot_send, tot_s, gs, num_s, co_f, co_a, co_b, co_send, co_recv,
     pf, r1_send, r1_recv, am,
-    d_send, d_recv, pin, pout, pick, table,
-    xring, acc_s, sq_s, ybuf, mixer, t_send, t_recv, r2_send, r2_recv, own,
+    d_send, d_recv, e_send, e_recv, am_next, pin, pout, pick, pick_next, table,
+    xring, acc_s, sq_s, ybuf, mixer, t_send, t_recv, r2_send, r2_recv, own, l_send, l_recv,
     load_sem, wx_send, wx_recv, row_ss, row_rs, tot_ss, tot_rs, co_sem, r1_ss, r1_rs,
-    d_ss, d_rs, x_ss, x_rs, t_ss, t_rs, r2_ss, r2_rs,
+    d_ss, d_rs, e_ss, e_rs, a_ss, a_rs, l_ss, l_rs, x_ss, x_rs, t_ss, t_rs, r2_ss, r2_rs,
 ):
     sp = lax.axis_index("sp")
     tp = lax.axis_index("tp")
@@ -66,6 +66,9 @@
     above = lax.rem(z + 1, NZ) * 2 + core
     below = lax.rem(z + NZ - 1, NZ) * 2 + core
     after = jnp.where(core == 0, above, below)
+    before = jnp.where(core == 0, below, above)
+    second_after = lax.rem(z + 2 * step, NZ) * 2 + core
+    second_before = lax.rem(z + 2 * (NZ - step), NZ) * 2 + core
     mate = z * 2 + 1 - core
     y, x = sp // NX, lax.rem(sp, NX)
 
@@ -77,7 +80,7 @@
             barrier, inc=1, device_id={"sp": lax.rem(sp + i, NSP), "tp": tp}, device_id_type=MESH
         )
 
-    for other in (above, below, mate):
+    for other in (above, below, mate, second_after, second_before):
         pl.semaphore_signal(barrier, inc=1, device_id={"sp": sp, "tp": other}, device_id_type=MESH)
 
     loads = [
@@ -163,10 +166,11 @@
         return pl.ds(pl.multiple_of(block * TOK, 8), TOK)
 
     place = iota((HROWS, ROWS), 1).astype(F32)
-    first, second = spots(table[block_rows(tp), :])
-    pick[...] = jnp.transpose(
-        jnp.where((place == first) | (place == second), 1.0, 0.0)
-    ).astype(BF16)
+    for target, block in ((pick, tp), (pick_next, after)):
+        first, second = spots(table[block_rows(block), :])
+        target[...] = jnp.transpose(
+            jnp.where((place == first) | (place == second), 1.0, 0.0)
+        ).astype(BF16)
 
     def reordered(outer, middle):
         n = iota((ROWS, 1), 0)
@@ -179,7 +183,7 @@
     pin[...] = reordered(PER, SLOT)
     pout[...] = reordered(SLOT, PER)
 
-    pl.semaphore_wait(barrier, NSP - 1 + 3)
+    pl.semaphore_wait(barrier, NSP - 1 + 5)
 
     def row_copy_x(i):
         return pltpu.make_async_remote_copy(
@@ -291,12 +295,13 @@
     swap.wait()
     both = jnp.concatenate([mine_b, co_recv[...]], axis=1)
 
-    @pl.loop(0, GROUPS)
-    def _(j):
-        at = pl.ds(pl.multiple_of(j * WIDE, WIDE), WIDE)
-        part = dot(both, wv[:, :, at].reshape(2 * HEAD_DIM, WIDE))
-        for i in range(NZ):
-            pf[i, pl.ds(pl.multiple_of(j * TOK, 8), TOK), :] = part[i * TOK : (i + 1) * TOK]
+    def project(h):
+        @pl.loop(h * GT, (h + 1) * GT)
+        def _(j):
+            at = pl.ds(pl.multiple_of(j * WIDE, WIDE), WIDE)
+            part = dot(both, wv[:, :, at].reshape(2 * HEAD_DIM, WIDE))
+            for i in range(NZ):
+                pf[i, pl.ds(pl.multiple_of(j * TOK, 8), TOK), :] = part[i * TOK : (i + 1) * TOK]
 
     srows = TROWS // STRIPES
 
@@ -326,6 +331,27 @@
 
     def slot_rows(s):
         return pl.ds(pl.multiple_of(s * SLOT, SLOT), SLOT)
+
+    def to_experts(h, chosen, tokens, sent, received, send_sem, recv_sem):
+        sent[h] = dot(chosen[...], tokens[h * HROWS : (h + 1) * HROWS]).astype(BF16)
+
+        @pl.loop(1, NSP)
+        def _(i):
+            to = lax.rem(sp + i, NSP)
+            pltpu.make_async_remote_copy(
+                src_ref=sent.at[h, slot_rows(to)], dst_ref=received.at[h, slot_rows(sp)],
+                send_sem=send_sem.at[h], recv_sem=recv_sem.at[h],
+                device_id={"sp": to, "tp": tp}, device_id_type=MESH,
+            ).start()
+
+        received[h, slot_rows(sp)] = sent[h, slot_rows(sp)]
+
+    def next_copy(h):
+        rows = pl.ds(h * HROWS, HROWS)
+        return pltpu.make_async_remote_copy(
+            src_ref=am.at[rows], dst_ref=am_next.at[rows], send_sem=a_ss.at[h], recv_sem=a_rs.at[h],
+            device_id={"sp": sp, "tp": before}, device_id_type=MESH,
+        )
 
     def dispatch(h):
         for p in (2 * h, 2 * h + 1):
@@ -342,27 +368,24 @@
                 axis=0,
             )
             am[rows] = (old + (pf[z, rows] + sides[0] + sides[1])).astype(BF16)
-        d_send[h] = dot(pick[...], am[h * HROWS : (h + 1) * HROWS]).astype(BF16)
-
-        @pl.loop(1, NSP)
-        def _(i):
-            to = lax.rem(sp + i, NSP)
-            pltpu.make_async_remote_copy(
-                src_ref=d_send.at[h, slot_rows(to)], dst_ref=d_recv.at[h, slot_rows(sp)],
-                send_sem=d_ss.at[h], recv_sem=d_rs.at[h],
-                device_id={"sp": to, "tp": tp}, device_id_type=MESH,
-            ).start()
-
-        d_recv[h, slot_rows(sp)] = d_send[h, slot_rows(sp)]
-
+        next_copy(h).start()
+        to_experts(h, pick, am, d_send, d_recv, d_ss, d_rs)
+
+    def relay(h):
+        next_copy(h).wait_recv()
+        to_experts(h, pick_next, am_next, e_send, e_recv, e_ss, e_rs)
+
+    project(0)
+    sum_steps(0, 0)
+    project(1)
     loads[4].wait()
-    sum_steps(0, 0)
     for m in range(1, 4):
         sum_steps(0, m)
         sum_steps(1, m - 1)
     dispatch(0)
     sum_steps(1, 3)
     dispatch(1)
+    relay(0)
 
     for load in loads[1:4]:
         load.wait()
@@ -387,24 +410,42 @@
         return pltpu.make_async_remote_copy(
             src_ref=r2_send.at[k, h], dst_ref=r2_recv.at[k + 1, h],
             send_sem=r2_ss.at[k, h], recv_sem=r2_rs.at[k + 1, h],
+            device_id={"sp": sp, "tp": jnp.where(k == NZ - 2, second_after, after)},
+            device_id_type=MESH,
+        )
+
+    def last_copy(h):
+        return pltpu.make_async_remote_copy(
+            src_ref=l_send.at[h], dst_ref=l_recv.at[h], send_sem=l_ss.at[h], recv_sem=l_rs.at[h],
             device_id={"sp": sp, "tp": after}, device_id_type=MESH,
         )
 
-    def arrive(k, h):
-        @pl.when(k == 0)
-        def _():
-            pltpu.make_async_copy(d_recv.at[h, others], d_recv.at[h, others], d_rs.at[h]).wait()
-            xring[0, h] = dot(pin[...], d_recv[h]).astype(BF16)
-
-        @pl.loop(0, PIECES)
-        def _(p):
-            @pl.when(k > 0)
-            def _():
-                row_copy(k - 1, h, p).wait_recv()
-
-            @pl.when(k < NZ - 1)
-            def _():
-                row_copy(k, h, p).start()
+    def from_plane(k, h, received, recv_sem):
+        pltpu.make_async_copy(received.at[h, others], received.at[h, others], recv_sem.at[h]).wait()
+        xring[k, h] = dot(pin[...], received[h]).astype(BF16)
+
+    def arrive(t, h):
+        k = jnp.where(t <= 2, t, t - 1)
+
+        @pl.when(t == 0)
+        def _():
+            from_plane(0, h, d_recv, d_rs)
+
+        @pl.when(t != 3)
+        def _():
+            @pl.loop(0, PIECES)
+            def _(p):
+                @pl.when(k > 0)
+                def _():
+                    row_copy(k - 1, h, p).wait_recv()
+
+                @pl.when(k < NZ - 2)
+                def _():
+                    row_copy(k, h, p).start()
+
+        @pl.when(t == 2)
+        def _():
+            from_plane(NZ - 1, h, e_recv, e_rs)
 
     def first_part(k, h):
         acc = jnp.zeros((PER, 4 * HEAD_DIM), F32)
@@ -466,42 +507,58 @@
         def _():
             own[h] = mixed
 
+        @pl.when(k == NZ - 1)
+        def _():
+            l_send[h] = mixed.astype(BF16)
+            last_copy(h).start()
+
         @pl.when(k == 1)
         def _():
             r2_send[k, h] = mixed.astype(BF16)
             total_copy(k, h).start()
 
-        @pl.when(k > 1)
+        @pl.when((k > 1) & (k < NZ - 1))
         def _():
             total_copy(k - 1, h).wait_recv()
             r2_send[k, h] = (mixed + r2_recv[k, h].astype(F32)).astype(BF16)
             total_copy(k, h).start()
 
     @pl.loop(0, NZ)
-    def _(k):
-        arrive(k, 0)
+    def _(t):
+        k = jnp.where(t < 2, t, jnp.where(t == 2, NZ - 1, t - 1))
+        back = jnp.where(t < 4, t - 2, jnp.where(t == 4, NZ - 1, t - 3))
+        arrive(t, 0)
         acc, squares = first_part(k, 0)
         acc_s[...] = acc
         sq_s[...] = squares
 
-        @pl.when(k > 0)
-        def _():
-            combine(k - 1, 0)
-
-        arrive(k, 1)
+        @pl.when(t == 0)
+        def _():
+            relay(1)
+
+        @pl.when(t >= 2)
+        def _():
+            combine(back, 0)
+
+        arrive(t, 1)
         acc, squares = first_part(k, 1)
         second_part(k, acc_s[...] + acc, sq_s[...] + squares)
 
-        @pl.when(k > 0)
-        def _():
-            combine(k - 1, 1)
+        @pl.when(t >= 2)
+        def _():
+            combine(back, 1)
+
+    @pl.loop(NZ - 3, NZ - 1)
+    def _(k):
+        for h in range(TURNS):
+            combine(k, h)
 
     for h in range(TURNS):
-        combine(NZ - 1, h)
+        last_copy(h).wait_recv()
     for h in range(TURNS):
-        total_copy(NZ - 1, h).wait_recv()
+        total_copy(NZ - 2, h).wait_recv()
         result = am[h * HROWS : (h + 1) * HROWS].astype(F32) + (
-            own[h] + r2_recv[NZ, h].astype(F32)
+            own[h] + l_recv[h].astype(F32) + r2_recv[NZ - 1, h].astype(F32)
         )
         for j in range(GT):
             at = slice((h * GT + j) * WIDE, (h * GT + j + 1) * WIDE)
@@ -512,7 +569,12 @@
             for m in range(hops(d, p)):
                 sum_copy(d, m, p).wait_send()
 
-    @pl.loop(1, NZ)
+    for h in range(TURNS):
+        next_copy(h).wait_send()
+        last_copy(h).wait_send()
+        pltpu.make_async_copy(e_send.at[h, others], e_send.at[h, others], e_ss.at[h]).wait()
+
+    @pl.loop(1, NZ - 1)
     def _(k):
         @pl.loop(0, TURNS)
         def _(h):
@@ -582,8 +644,12 @@
             pltpu.VMEM((TROWS, WIDE), BF16),
             pltpu.VMEM((TURNS, ROWS, WIDE), BF16),
             pltpu.VMEM((TURNS, ROWS, WIDE), BF16),
+            pltpu.VMEM((TURNS, ROWS, WIDE), BF16),
+            pltpu.VMEM((TURNS, ROWS, WIDE), BF16),
+            pltpu.VMEM((TROWS, WIDE), BF16),
             pltpu.VMEM((ROWS, ROWS), BF16),
             pltpu.VMEM((ROWS, ROWS), BF16),
+            pltpu.VMEM((ROWS, HROWS), BF16),
             pltpu.VMEM((ROWS, HROWS), BF16),
             pltpu.VMEM((LEN, HEAD_DIM), F32),
             pltpu.VMEM((NZ, TURNS, ROWS, WIDE), BF16),
@@ -594,13 +660,16 @@
             pltpu.VMEM((NZ, TURNS, ROWS, WIDE), BF16),
             pltpu.VMEM((NZ, TURNS, ROWS, WIDE), BF16),
             pltpu.VMEM((NZ, TURNS, HROWS, WIDE), BF16),
-            pltpu.VMEM((NZ + 1, TURNS, HROWS, WIDE), BF16),
+            pltpu.VMEM((NZ, TURNS, HROWS, WIDE), BF16),
             pltpu.VMEM((TURNS, HROWS, WIDE), F32),
+            pltpu.VMEM((TURNS, HROWS, WIDE), BF16),
+            pltpu.VMEM((TURNS, HROWS, WIDE), BF16),
             dma((5,)), dma((4,)), dma((4,)), dma((NX,)), dma((NX,)), dma((NX,)), dma((NX,)), dma((2,)),
             dma((2, 4, STRIPES)), dma((2, 4, STRIPES)),
-            dma((TURNS,)), dma((TURNS,)),
-            dma((NZ - 1, TURNS, PIECES)), dma((NZ - 1, TURNS, PIECES)),
-            dma((NZ, TURNS)), dma((NZ, TURNS)), dma((NZ, TURNS)), dma((NZ + 1, TURNS)),
+            dma((TURNS,)), dma((TURNS,)), dma((TURNS,)), dma((TURNS,)),
+            dma((TURNS,)), dma((TURNS,)), dma((TURNS,)), dma((TURNS,)),
+            dma((NZ - 2, TURNS, PIECES)), dma((NZ - 2, TURNS, PIECES)),
+            dma((NZ, TURNS)), dma((NZ, TURNS)), dma((NZ, TURNS)), dma((NZ, TURNS)),
         ],
         compiler_params=pltpu.CompilerParams(
             collective_id=0, has_side_effects=True, vmem_limit_bytes=60 << 20

time: 139 us -> 138 us (level)
  no operation moved by 1% of the time
where the time goes in v3:
time: 138 us
  Pallas kernels  136 us (99%)
  local copies, waits for them, and re-layouts  1.62 us (1%)
    pallas_call x1, Pallas kernels, local(): pl.pallas_call(kernel, name='layer', out_shape=jax.ShapeDtypeStruct((TOK,...  136 us

profile of v3, /device:TPU:32, one launch (start us, length us, event | category | flops | bytes accessed | tf_op | source)
XLA Modules:
  0.0 137.7 jit_solution(12196716717506308810)
XLA Ops:
  0.0 136.1 %layer.1 = bf16[24,4096]{1,0:T(8,128)(2,1)} custom-call(bf16[384,128]{1,0:T(8,128)(2,1)} %q_ref.1, bf16[384,128]{1,0:T(8,128)(2,1)} %k_ref.1, bf16[384,128]{1,0:T(8,128)(2,1)} %v_ref.1, bf16[384,128]{1,0:T(8,128)(2,1)} %og_ref.1, f32[1,384]{1,0:T(1,128)} %ig_ref.1, f32[1,384]{1,0:T(1,128)} %fg_ref.1, f32[1,384]{1,0:T(1,128)} %ex_ref.1, f32[1,128]{1,0:T(1,128)} %bitcast.13, ...), custom_call_target="tpu_custom_call" | custom-call | tf_op jit(solution)/shard_map/layer/pallas_call | solution.py:620
  136.1 1.6 %copy.18 = bf16[24,4096]{1,0:T(8,128)(2,1)} copy(bf16[24,4096]{1,0:T(8,128)(2,1)} %layer.1) | data formatting | bytes 393216

commit v4 on v2

--- a/solution.py
+++ b/solution.py
@@ -25,6 +25,7 @@
 HROWS = GT * TOK
 PER = ROWS // GT
 NX = 4
+LAG = 2
 PIECES = 2
 STRIPES = 4
 
@@ -53,10 +54,10 @@
     wv, gw, dn, resid,
     row_s, tot_send, tot_s, gs, num_s, co_f, co_a, co_b, co_send, co_recv,
     pf, r1_send, r1_recv, am,
-    d_send, d_recv, pin, pout, pick, table,
+    d_send, d_recv, am_next, pin, pout, pick, pick_next, table,
     xring, acc_s, sq_s, ybuf, mixer, t_send, t_recv, r2_send, r2_recv, own,
     load_sem, wx_send, wx_recv, row_ss, row_rs, tot_ss, tot_rs, co_sem, r1_ss, r1_rs,
-    d_ss, d_rs, x_ss, x_rs, t_ss, t_rs, r2_ss, r2_rs,
+    d_ss, d_rs, a_sem, x_ss, x_rs, t_ss, t_rs, r2_ss, r2_rs,
 ):
     sp = lax.axis_index("sp")
     tp = lax.axis_index("tp")
@@ -66,6 +67,7 @@
     above = lax.rem(z + 1, NZ) * 2 + core
     below = lax.rem(z + NZ - 1, NZ) * 2 + core
     after = jnp.where(core == 0, above, below)
+    before = jnp.where(core == 0, below, above)
     mate = z * 2 + 1 - core
     y, x = sp // NX, lax.rem(sp, NX)
 
@@ -163,10 +165,11 @@
         return pl.ds(pl.multiple_of(block * TOK, 8), TOK)
 
     place = iota((HROWS, ROWS), 1).astype(F32)
-    first, second = spots(table[block_rows(tp), :])
-    pick[...] = jnp.transpose(
-        jnp.where((place == first) | (place == second), 1.0, 0.0)
-    ).astype(BF16)
+    for target, block in ((pick, tp), (pick_next, after)):
+        first, second = spots(table[block_rows(block), :])
+        target[...] = jnp.transpose(
+            jnp.where((place == first) | (place == second), 1.0, 0.0)
+        ).astype(BF16)
 
     def reordered(outer, middle):
         n = iota((ROWS, 1), 0)
@@ -291,12 +294,13 @@
     swap.wait()
     both = jnp.concatenate([mine_b, co_recv[...]], axis=1)
 
-    @pl.loop(0, GROUPS)
-    def _(j):
-        at = pl.ds(pl.multiple_of(j * WIDE, WIDE), WIDE)
-        part = dot(both, wv[:, :, at].reshape(2 * HEAD_DIM, WIDE))
-        for i in range(NZ):
-            pf[i, pl.ds(pl.multiple_of(j * TOK, 8), TOK), :] = part[i * TOK : (i + 1) * TOK]
+    def project(h):
+        @pl.loop(h * GT, (h + 1) * GT)
+        def _(j):
+            at = pl.ds(pl.multiple_of(j * WIDE, WIDE), WIDE)
+            part = dot(both, wv[:, :, at].reshape(2 * HEAD_DIM, WIDE))
+            for i in range(NZ):
+                pf[i, pl.ds(pl.multiple_of(j * TOK, 8), TOK), :] = part[i * TOK : (i + 1) * TOK]
 
     srows = TROWS // STRIPES
 
@@ -326,6 +330,26 @@
 
     def slot_rows(s):
         return pl.ds(pl.multiple_of(s * SLOT, SLOT), SLOT)
+
+    def to_experts(n, chosen, tokens):
+        d_send[n] = dot(chosen[...], tokens).astype(BF16)
+
+        @pl.loop(1, NSP)
+        def _(i):
+            to = lax.rem(sp + i, NSP)
+            pltpu.make_async_remote_copy(
+                src_ref=d_send.at[n, slot_rows(to)], dst_ref=d_recv.at[n, slot_rows(sp)],
+                send_sem=d_ss.at[n], recv_sem=d_rs.at[n],
+                device_id={"sp": to, "tp": tp}, device_id_type=MESH,
+            ).start()
+
+        d_recv[n, slot_rows(sp)] = d_send[n, slot_rows(sp)]
+
+    next_copy = pltpu.make_async_remote_copy(
+        src_ref=am.at[pl.ds(0, HROWS)], dst_ref=am_next,
+        send_sem=a_sem.at[0], recv_sem=a_sem.at[1],
+        device_id={"sp": sp, "tp": before}, device_id_type=MESH,
+    )
 
     def dispatch(h):
         for p in (2 * h, 2 * h + 1):
@@ -342,21 +366,14 @@
                 axis=0,
             )
             am[rows] = (old + (pf[z, rows] + sides[0] + sides[1])).astype(BF16)
-        d_send[h] = dot(pick[...], am[h * HROWS : (h + 1) * HROWS]).astype(BF16)
-
-        @pl.loop(1, NSP)
-        def _(i):
-            to = lax.rem(sp + i, NSP)
-            pltpu.make_async_remote_copy(
-                src_ref=d_send.at[h, slot_rows(to)], dst_ref=d_recv.at[h, slot_rows(sp)],
-                send_sem=d_ss.at[h], recv_sem=d_rs.at[h],
-                device_id={"sp": to, "tp": tp}, device_id_type=MESH,
-            ).start()
-
-        d_recv[h, slot_rows(sp)] = d_send[h, slot_rows(sp)]
-
+        if h == 0:
+            next_copy.start()
+        to_experts(h, pick, am[h * HROWS : (h + 1) * HROWS])
+
+    project(0)
+    sum_steps(0, 0)
+    project(1)
     loads[4].wait()
-    sum_steps(0, 0)
     for m in range(1, 4):
         sum_steps(0, m)
         sum_steps(1, m - 1)
@@ -364,6 +381,9 @@
     sum_steps(1, 3)
     dispatch(1)
 
+    next_copy.wait_recv()
+    to_experts(TURNS, pick_next, am_next[...])
+
     for load in loads[1:4]:
         load.wait()
     for copy in shared[1:]:
@@ -390,21 +410,31 @@
             device_id={"sp": sp, "tp": after}, device_id_type=MESH,
         )
 
+    def from_plane(k, h, n):
+        pltpu.make_async_copy(d_recv.at[n, others], d_recv.at[n, others], d_rs.at[n]).wait()
+        xring[k, h] = dot(pin[...], d_recv[n]).astype(BF16)
+
     def arrive(k, h):
         @pl.when(k == 0)
         def _():
-            pltpu.make_async_copy(d_recv.at[h, others], d_recv.at[h, others], d_rs.at[h]).wait()
-            xring[0, h] = dot(pin[...], d_recv[h]).astype(BF16)
+            from_plane(0, h, h)
+
+        last = NZ - 2 if h == 0 else NZ - 1
 
         @pl.loop(0, PIECES)
         def _(p):
-            @pl.when(k > 0)
+            @pl.when((k > 0) & (k <= last))
             def _():
                 row_copy(k - 1, h, p).wait_recv()
 
-            @pl.when(k < NZ - 1)
+            @pl.when(k < last)
             def _():
                 row_copy(k, h, p).start()
+
+        if h == 0:
+            @pl.when(k == NZ - 1)
+            def _():
+                from_plane(NZ - 1, h, TURNS)
 
     def first_part(k, h):
         acc = jnp.zeros((PER, 4 * HEAD_DIM), F32)
@@ -484,20 +514,23 @@
         acc_s[...] = acc
         sq_s[...] = squares
 
-        @pl.when(k > 0)
+        @pl.when(k >= LAG)
         def _():
-            combine(k - 1, 0)
+            combine(k - LAG, 0)
 
         arrive(k, 1)
         acc, squares = first_part(k, 1)
         second_part(k, acc_s[...] + acc, sq_s[...] + squares)
 
-        @pl.when(k > 0)
+        @pl.when(k >= LAG)
         def _():
-            combine(k - 1, 1)
-
-    for h in range(TURNS):
-        combine(NZ - 1, h)
+            combine(k - LAG, 1)
+
+    @pl.loop(NZ - LAG, NZ)
+    def _(k):
+        for h in range(TURNS):
+            combine(k, h)
+
     for h in range(TURNS):
         total_copy(NZ - 1, h).wait_recv()
         result = am[h * HROWS : (h + 1) * HROWS].astype(F32) + (
@@ -518,14 +551,20 @@
         def _(h):
             total_copy(k, h).wait_send()
 
-            @pl.loop(0, PIECES)
-            def _(p):
-                row_copy(k - 1, h, p).wait_send()
+            @pl.when((h > 0) | (k < NZ - 1))
+            def _():
+                @pl.loop(0, PIECES)
+                def _(p):
+                    row_copy(k - 1, h, p).wait_send()
+
+    next_copy.wait_send()
+
+    @pl.loop(0, TURNS + 1)
+    def _(n):
+        pltpu.make_async_copy(d_send.at[n, others], d_send.at[n, others], d_ss.at[n]).wait()
 
     @pl.loop(0, TURNS)
     def _(h):
-        pltpu.make_async_copy(d_send.at[h, others], d_send.at[h, others], d_ss.at[h]).wait()
-
         @pl.loop(0, NZ)
         def _(k):
             pltpu.make_async_copy(
@@ -580,10 +619,12 @@
             pltpu.VMEM((2, 4, TROWS, WIDE), BF16),
             pltpu.VMEM((2, 4, TROWS, WIDE), BF16),
             pltpu.VMEM((TROWS, WIDE), BF16),
-            pltpu.VMEM((TURNS, ROWS, WIDE), BF16),
-            pltpu.VMEM((TURNS, ROWS, WIDE), BF16),
+            pltpu.VMEM((TURNS + 1, ROWS, WIDE), BF16),
+            pltpu.VMEM((TURNS + 1, ROWS, WIDE), BF16),
+            pltpu.VMEM((HROWS, WIDE), BF16),
             pltpu.VMEM((ROWS, ROWS), BF16),
             pltpu.VMEM((ROWS, ROWS), BF16),
+            pltpu.VMEM((ROWS, HROWS), BF16),
             pltpu.VMEM((ROWS, HROWS), BF16),
             pltpu.VMEM((LEN, HEAD_DIM), F32),
             pltpu.VMEM((NZ, TURNS, ROWS, WIDE), BF16),
@@ -598,7 +639,7 @@
             pltpu.VMEM((TURNS, HROWS, WIDE), F32),
             dma((5,)), dma((4,)), dma((4,)), dma((NX,)), dma((NX,)), dma((NX,)), dma((NX,)), dma((2,)),
             dma((2, 4, STRIPES)), dma((2, 4, STRIPES)),
-            dma((TURNS,)), dma((TURNS,)),
+            dma((TURNS + 1,)), dma((TURNS + 1,)), dma((2,)),
             dma((NZ - 1, TURNS, PIECES)), dma((NZ - 1, TURNS, PIECES)),
             dma((NZ, TURNS)), dma((NZ, TURNS)), dma((NZ, TURNS)), dma((NZ + 1, TURNS)),
         ],

time: 139 us -> 135 us (0.971)
  Pallas kernels: 137 us -> 133 us
    pallas_call x1, Pallas kernels: 137 us -> 133 us  [local(): pl.pallas_call(kernel, name='layer', out_shape=jax.ShapeDtypeStruct((TOK,...]
where the time goes in v4:
time: 135 us
  Pallas kernels  133 us (99%)
  local copies, waits for them, and re-layouts  1.62 us (1%)
    pallas_call x1, Pallas kernels, local(): pl.pallas_call(kernel, name='layer', out_shape=jax.ShapeDtypeStruct((TOK,...  133 us

profile of v4, /device:TPU:32, one launch (start us, length us, event | category | flops | bytes accessed | tf_op | source)
XLA Modules:
  0.0 134.9 jit_solution(15855716059392487427)
XLA Ops:
  0.0 133.3 %layer.1 = bf16[24,4096]{1,0:T(8,128)(2,1)} custom-call(bf16[384,128]{1,0:T(8,128)(2,1)} %q_ref.1, bf16[384,128]{1,0:T(8,128)(2,1)} %k_ref.1, bf16[384,128]{1,0:T(8,128)(2,1)} %v_ref.1, bf16[384,128]{1,0:T(8,128)(2,1)} %og_ref.1, f32[1,384]{1,0:T(1,128)} %ig_ref.1, f32[1,384]{1,0:T(1,128)} %fg_ref.1, f32[1,384]{1,0:T(1,128)} %ex_ref.1, f32[1,128]{1,0:T(1,128)} %bitcast.13, ...), custom_call_target="tpu_custom_call" | custom-call | tf_op jit(solution)/shard_map/layer/pallas_call | solution.py:597
  133.3 1.6 %copy.18 = bf16[24,4096]{1,0:T(8,128)(2,1)} copy(bf16[24,4096]{1,0:T(8,128)(2,1)} %layer.1) | data formatting | bytes 393216

commit v5 on v4

--- a/solution.py
+++ b/solution.py
@@ -514,16 +514,13 @@
         acc_s[...] = acc
         sq_s[...] = squares
 
+        arrive(k, 1)
+        acc, squares = first_part(k, 1)
+        second_part(k, acc_s[...] + acc, sq_s[...] + squares)
+
         @pl.when(k >= LAG)
         def _():
             combine(k - LAG, 0)
-
-        arrive(k, 1)
-        acc, squares = first_part(k, 1)
-        second_part(k, acc_s[...] + acc, sq_s[...] + squares)
-
-        @pl.when(k >= LAG)
-        def _():
             combine(k - LAG, 1)
 
     @pl.loop(NZ - LAG, NZ)

time: 135 us -> 134 us (level)
  no operation moved by 1% of the time
where the time goes in v5:
time: 134 us
  Pallas kernels  132 us (99%)
  local copies, waits for them, and re-layouts  1.62 us (1%)
    pallas_call x1, Pallas kernels, local(): pl.pallas_call(kernel, name='layer', out_shape=jax.ShapeDtypeStruct((TOK,...  132 us

profile of v5, /device:TPU:32, one launch (start us, length us, event | category | flops | bytes accessed | tf_op | source)
XLA Modules:
  0.0 133.8 jit_solution(11809483260417031910)
XLA Ops:
  0.0 132.2 %layer.1 = bf16[24,4096]{1,0:T(8,128)(2,1)} custom-call(bf16[384,128]{1,0:T(8,128)(2,1)} %q_ref.1, bf16[384,128]{1,0:T(8,128)(2,1)} %k_ref.1, bf16[384,128]{1,0:T(8,128)(2,1)} %v_ref.1, bf16[384,128]{1,0:T(8,128)(2,1)} %og_ref.1, f32[1,384]{1,0:T(1,128)} %ig_ref.1, f32[1,384]{1,0:T(1,128)} %fg_ref.1, f32[1,384]{1,0:T(1,128)} %ex_ref.1, f32[1,128]{1,0:T(1,128)} %bitcast.13, ...), custom_call_target="tpu_custom_call" | custom-call | tf_op jit(solution)/shard_map/layer/pallas_call | solution.py:594
  132.2 1.6 %copy.18 = bf16[24,4096]{1,0:T(8,128)(2,1)} copy(bf16[24,4096]{1,0:T(8,128)(2,1)} %layer.1) | data formatting | bytes 393216
